TPU v7x, 256 devices: a whole 4x4x8 slice. The times are simulated.
256 devices in a mesh: ep: 64 (over z, y, core), tp: 4 (over x).
Axes of the slice: x: 4, y: 4, z: 8, core: 2. Of those that a mesh axis runs over, the one named last changes fastest.
Arguments:
- tokens: bfloat16 [3072, 2048], P('ep'), may hold values from -6 to 6
- out_grad: bfloat16 [3072, 2048], P('ep'), may hold values from -4 to 4
- expert_ids: int32 [3072, 4], P('ep'), may hold values from 0 to 63, all different within a row; in each aligned block of 48 rows (0 to 47, 48 to 95, ...) at most 8 rows name the same one
- router_weight: bfloat16 [2048, 64], replicated, may hold values from -0.125 to 0.125
- w_gate: bfloat16 [64, 2048, 1536], P('ep', None, 'tp'), may hold values from -0.125 to 0.125
- w_up: bfloat16 [64, 2048, 1536], P('ep', None, 'tp'), may hold values from -0.125 to 0.125
- w_down: bfloat16 [64, 1536, 2048], P('ep', 'tp'), may hold values from -0.15625 to 0.15625
Outputs:
- token_grad: bfloat16 [3072, 2048], P('ep', 'tp')
- router_grad: float32 [2048, 64], P('tp', 'ep')
- w_gate_grad: bfloat16 [64, 2048, 1536], P('ep', None, 'tp')
- w_up_grad: bfloat16 [64, 2048, 1536], P('ep', None, 'tp')
- w_down_grad: bfloat16 [64, 1536, 2048], P('ep', 'tp')
Inputs may be any that keep to these rules, and one draw needn't show every extreme that they name: `expert_ids`: each row names 4 different experts; among the rows of one device no expert is named more than 8 times, and in some devices' rows one expert is named exactly 8 times.
All inputs are finite; a program needn't handle non-finite values.
Results may differ from a plain program's by a relative error of at most 0.0058.
Values may be sent and summed in bfloat16 or wider, within the bound.
No kernel may reach another device: no remote copies, remote signals or barrier semaphores. Data moves between devices by JAX's collectives and lax.ppermute only.
A program may use at most 128 MiB of HBM per device.

v0:
```python
import functools

import jax
import jax.numpy as jnp
from jax import lax
from jax.experimental import pallas as pl
from jax.experimental.pallas import tpu as pltpu
from jax.sharding import PartitionSpec as P


F32 = jnp.float32
BF16 = jnp.bfloat16
HI = lax.Precision.HIGHEST
VMEM = pl.BlockSpec(memory_space=pltpu.VMEM)
SMEM = pl.BlockSpec(memory_space=pltpu.SMEM)


def mm(a, b, dims, precision=None):
    return lax.dot_general(a, b, (dims, ((), ())), precision=precision, preferred_element_type=F32)


NN = ((1,), (0,))
NT = ((1,), (1,))
TN = ((0,), (0,))


def iota(shape, dim):
    return lax.broadcasted_iota(jnp.int32, shape, dim)


def bits(cap):
    return cap.bit_length() - 1


def spread(experts, cap):
    rows = experts * cap
    return ((iota((rows, experts), 0) >> bits(cap)) == iota((rows, experts), 1)).astype(F32)


def dispatch_kernel(cap, tp_ref, tok_ref, og_ref, ids_ref, rw_ref, send_ref, code_ref, gate_ref, mine_ref):
    n_tok = tok_ref.shape[0]
    experts = rw_ref.shape[0]
    share = send_ref.shape[1] // 2
    start = pl.multiple_of(tp_ref[0] * share, share)
    logits = mm(tok_ref[...], rw_ref[...], NT)
    ids = ids_ref[...].astype(F32).T
    lane = iota((n_tok, experts), 1).astype(F32)
    hit = lane == ids[:, 0:1]
    for k in range(1, ids.shape[1]):
        hit = hit | (lane == ids[:, k : k + 1])
    mask = hit.astype(F32)
    top = jnp.max(jnp.where(hit, logits, -jnp.inf), axis=1, keepdims=True)
    weight = jnp.where(hit, jnp.exp(jnp.where(hit, logits - top, 0.0)), 0.0)
    gate = weight / jnp.sum(weight, axis=1, keepdims=True)
    earlier = (iota((n_tok, n_tok), 1) < iota((n_tok, n_tok), 0)).astype(BF16)
    rank = mm(earlier, mask.astype(BF16), NN)
    code = mask * (rank + 1.0)
    code_ref[...] = code
    gate_ref[...] = gate
    expand = spread(experts, cap).astype(BF16)
    rows = experts * cap
    code_of = mm(expand, code.astype(BF16), NT)
    pick = code_of == ((iota((rows, n_tok), 0) & (cap - 1)) + 1).astype(F32)
    gate_of, rest = None, gate
    for _ in range(3):
        piece = rest.astype(BF16)
        rest = rest - piece.astype(F32)
        term = mm(expand, piece, NT)
        gate_of = term if gate_of is None else gate_of + term
    gate_of = jnp.sum(jnp.where(pick, gate_of, 0.0), axis=1, keepdims=True)
    mine = tok_ref[:, pl.ds(start, share)]
    mine_ref[...] = mine
    both = mm(pick.astype(F32).astype(BF16), jnp.concatenate([mine, og_ref[:, pl.ds(start, share)]], axis=1), NN)
    send_ref[:, :share] = both[:, :share].astype(BF16)
    send_ref[:, share:] = (both[:, share:] * gate_of).astype(BF16)


LEFT, RIGHT = 0, 1


def joined(refs, side):
    share = refs[0].shape[1] // 2
    return jnp.concatenate([r[:, side * share : (side + 1) * share] for r in refs], axis=0)


def block(tp_ref, off, share):
    return pl.ds(pl.multiple_of(lax.rem(tp_ref[0] + off, 4) * share, share), share)


def forward(tp_ref, groups, share, wgu, wd, start=None):
    total = start
    for off, refs in groups:
        at = block(tp_ref, off, share)
        terms = (mm(joined(refs, LEFT), wgu[at, :], NN), mm(joined(refs, RIGHT), wd[:, at], NT))
        total = terms if total is None else tuple(a + b for a, b in zip(total, terms))
    return total


def units(cap, both_pre, back):
    rows, ff = back.shape
    gate_pre, up_pre = both_pre[:, :ff], both_pre[:, ff:]
    glu = jnp.minimum(gate_pre, 7.0)
    linear = jnp.clip(up_pre, -7.0, 7.0)
    sig = jax.nn.sigmoid(1.702 * glu)
    act = glu * sig
    hidden = (linear + 1.0) * act
    slope = (linear + 1.0) * (sig + 1.702 * glu * sig * (1.0 - sig))
    slope = jnp.where(gate_pre < 7.0, slope, 0.0)
    up_slope = jnp.where((up_pre > -7.0) & (up_pre < 7.0), act, 0.0)
    score = jnp.sum(hidden * back, axis=1, keepdims=True)
    peers = rows // cap
    spot = ((iota((rows, 128), 0) & (cap - 1)) == iota((rows, 128), 1)).astype(F32) * score
    group = ((iota((peers, rows), 1) >> bits(cap)) == iota((peers, rows), 0)).astype(F32)
    grads = jnp.concatenate([(back * slope).astype(BF16), (back * up_slope).astype(BF16)], axis=1)
    return hidden.astype(BF16), grads, mm(group, spot, NN, HI)


def near_kernel(tp_ref, own, pa, pb, na, nb, wgu, wd, pre, bk):
    groups = ((0, (own,)), (3, (pa, pb)), (1, (na, nb)))
    pre[...], bk[...] = forward(tp_ref, groups, own.shape[1] // 2, wgu, wd)


def far_kernel(cap, tp_ref, f0, f1, pre, bk, wgu, wd, hid, grads, score, b2a, b2b):
    share = f0.shape[1] // 2
    half = f0.shape[0]
    start = (pre[...], bk[...])
    hid[...], values, score[...] = units(cap, *forward(tp_ref, ((2, (f0, f1)),), share, wgu, wd, start))
    grads[...] = values
    far = mm(values, wgu[block(tp_ref, 2, share), :], NT).astype(BF16)
    b2a[...] = far[:half]
    b2b[...] = far[half:]


def token_kernel(tp_ref, grads_ref, wgu, b1a, b1b, b3a, b3b, b0):
    share = b0.shape[1]
    half = b0.shape[0] // 2
    grads = grads_ref[...]

    def part(off):
        return mm(grads, wgu[block(tp_ref, off, share), :], NT)

    ahead = part(1)
    b1a[...] = ahead[:half]
    b1b[...] = ahead[half:].astype(BF16)
    behind = part(3)
    b3a[...] = behind[:half].astype(BF16)
    b3b[...] = behind[half:]
    b0[...] = part(0)


def total_kernel(a, b, c, d, out):
    out[...] = a[...] + b[...] + c[...] + d[...]


def onward_kernel(b1a, s1, b3b, s2, ahead, behind):
    ahead[...] = (b1a[...] + s1[...].astype(F32)).astype(BF16)
    behind[...] = (b3b[...] + s2[...].astype(F32)).astype(BF16)


def weight_kernel(tp_ref, own, pa, pb, na, nb, f0, f1, hid, grads, d_logits_ref, rw_ref,
                  gwg_ref, gwu_ref, gwd_ref, part_ref):
    share = own.shape[1] // 2
    ff = gwg_ref.shape[1]
    part_ref[...] = mm(d_logits_ref[...], rw_ref[:, block(tp_ref, 0, share)].astype(F32), NN, HI)
    for off, refs in ((0, (own,)), (3, (pa, pb)), (1, (na, nb)), (2, (f0, f1))):
        at = block(tp_ref, off, share)
        t, g = joined(refs, LEFT), joined(refs, RIGHT)
        both = mm(t, grads[...], TN).astype(BF16)
        gwg_ref[at, :] = both[:, :ff]
        gwu_ref[at, :] = both[:, ff:]
        gwd_ref[:, at] = mm(hid[...], g, TN).astype(BF16)


def router_kernel(cap, q_ref, code_ref, gate_ref, tok_ref, *refs):
    (b0, d1, d2, e1, e2), (payload_ref, d_logits_ref) = refs[:5], refs[5:]
    rows, share = b0.shape
    half = rows // 2
    for i, (near, far) in enumerate(((d2, e1), (d1, e2))):
        n = half // cap
        value = b0[i * half : (i + 1) * half] + near[...].astype(F32) + far[...].astype(F32)
        payload_ref[pl.ds(i * n, n), :, :share] = value.astype(BF16).reshape(n, cap, share)
    code, gate = code_ref[...], gate_ref[...]
    q = q_ref[...].T
    score = jnp.zeros_like(code)
    for r in range(cap):
        score = score + jnp.where(code == r + 1.0, q[r : r + 1, :], 0.0)
    d_logits = score - gate * jnp.sum(score, axis=1, keepdims=True)
    d_logits_ref[...] = d_logits
    term = mm(d_logits, tok_ref[...].astype(F32), TN, HI)
    high = term.astype(BF16)
    low = (term - high.astype(F32)).astype(BF16)
    pieces = share // 128
    for j in range(pieces):
        payload_ref[:, j, share:] = high[:, j * 128 : (j + 1) * 128]
        payload_ref[:, pieces + j, share:] = low[:, j * 128 : (j + 1) * 128]


def mark_kernel(given, out):
    out[...] = given[...]


def home_kernel(cap, home_ref, code_ref, part_ref, tok_out_ref, router_ref):
    share = part_ref.shape[1]
    code = code_ref[...]
    n_tok, experts = code.shape
    rows = experts * cap
    code_of = mm(code.astype(BF16), spread(experts, cap).astype(BF16), NT)
    pick = code_of == ((iota((n_tok, rows), 1) & (cap - 1)) + 1).astype(F32)
    flat = home_ref[...].reshape(rows, home_ref.shape[2])
    tok_out_ref[...] = (
        mm(pick.astype(F32).astype(BF16), flat[:, :share], NN) + part_ref[...]
    ).astype(BF16)
    both = jnp.sum(home_ref[:, :, share:].astype(F32), axis=0)
    pieces = share // 128
    router_ref[...] = both[:pieces] + both[pieces:]


def cost(flops, data):
    return pl.CostEstimate(flops=flops, bytes_accessed=data, transcendentals=0)


def call(body, outs, flops, scalar=True, to_hbm=0, raw=()):
    def place(i, x):
        return pltpu.with_memory_space_constraint(x, pltpu.HBM if i in raw else pltpu.VMEM)

    def run(*args):
        ins = args[1:] if scalar else args
        return pl.pallas_call(
            body,
            out_shape=outs[:to_hbm] + [pltpu.VMEM(o.shape, o.dtype) for o in outs[to_hbm:]],
            in_specs=([SMEM] if scalar else []) + [VMEM] * len(ins),
            out_specs=[VMEM] * len(outs),
            cost_estimate=cost(flops, 4 << 20),
            compiler_params=pltpu.CompilerParams(vmem_limit_bytes=24 << 20),
        )(*args[: len(args) - len(ins)], *(place(i, x) for i, x in enumerate(ins)))

    return run


def shape(dims, dtype):
    return jax.ShapeDtypeStruct(dims, dtype)


def per_device(tokens, out_grad, expert_ids, router_weight, w_gate, w_up, w_down):
    n_tok, width = tokens.shape
    experts = router_weight.shape[1]
    peers = lax.axis_size("ep")
    tp = lax.axis_size("tp")
    cap = 8
    share = width // tp
    ff = w_gate.shape[2]
    rows = peers * cap
    half = rows // 2
    me = jnp.full((1,), lax.axis_index("tp"), jnp.int32)
    unit = 2 * rows * share * ff
    router_t = router_weight.T

    def hop(value, by):
        return lax.ppermute(value, "tp", [(i, (i + by) % tp) for i in range(tp)])

    def exchange(value):
        return lax.all_to_all(value, "ep", split_axis=0, concat_axis=0, tiled=True)

    send, code, gate, mine = call(
        functools.partial(dispatch_kernel, cap),
        [shape((rows, 2 * share), BF16), shape((n_tok, experts), F32), shape((n_tok, experts), F32),
         shape((n_tok, share), BF16)],
        unit,
        raw=(0, 1, 2, 3),
    )(me, tokens, out_grad, expert_ids.T, router_t)
    own = exchange(send.reshape(peers, cap, 2 * share)).reshape(rows, 2 * share)
    pa, nb = hop(own[:half], 1), hop(own[half:], -1)
    pb, na = hop(own[half:], 1), hop(own[:half], -1)
    f0, f1 = hop(pa, 1), hop(nb, -1)

    def load_kernel(wg, wu, wd, wgu_out, wd_out, sems):
        copies = [
            pltpu.make_async_copy(wg, wgu_out.at[:, :ff], sems.at[0]),
            pltpu.make_async_copy(wu, wgu_out.at[:, ff:], sems.at[1]),
            pltpu.make_async_copy(wd, wd_out, sems.at[2]),
        ]
        for copy in copies:
            copy.start()
        for copy in copies:
            copy.wait()

    wgu, wd = pl.pallas_call(
        load_kernel,
        out_shape=[pltpu.VMEM((width, 2 * ff), BF16), pltpu.VMEM((ff, width), BF16)],
        in_specs=[pl.BlockSpec(memory_space=pl.ANY)] * 3,
        out_specs=[VMEM] * 2,
        scratch_shapes=[pltpu.SemaphoreType.DMA((3,))],
        cost_estimate=cost(unit, 4 << 20),
        compiler_params=pltpu.CompilerParams(vmem_limit_bytes=24 << 20),
    )(*(pltpu.with_memory_space_constraint(w[0], pltpu.HBM) for w in (w_gate, w_up, w_down)))

    near = call(
        near_kernel, [shape((rows, 2 * ff), F32), shape((rows, ff), F32)], 9 * unit
    )(me, own, pa, pb, na, nb, wgu, wd)
    hid, grads, score, b2a, b2b = call(
        functools.partial(far_kernel, cap),
        [shape((rows, ff), BF16), shape((rows, 2 * ff), BF16), shape((peers, 128), F32)]
        + [shape((half, share), BF16)] * 2,
        5 * unit,
    )(me, f0, f1, *near, wgu, wd)
    s1, s2 = hop(b2a, 1), hop(b2b, -1)
    b1a, b1b, b3a, b3b, b0 = call(
        token_kernel,
        [shape((half, share), F32), shape((half, share), BF16), shape((half, share), BF16),
         shape((half, share), F32), shape((rows, share), F32)],
        6 * unit,
    )(me, grads, wgu)
    d1, d2 = hop(b1b, 1), hop(b3a, -1)
    ahead, behind = call(onward_kernel, [shape((half, share), BF16)] * 2, 1, scalar=False)(b1a, s1, b3b, s2)
    e1, e2 = hop(ahead, 1), hop(behind, -1)
    (gate,) = call(mark_kernel, [shape((n_tok, experts), F32)], 1, scalar=False)(gate)
    (score,) = call(total_kernel, [shape((peers, 128), F32)], 1, scalar=False)(
        score, hop(score, 1), hop(score, -1), hop(score, 2)
    )
    q = exchange(score.reshape(peers, 1, 128)).reshape(peers, 128)
    payload, d_logits = call(
        functools.partial(router_kernel, cap),
        [shape((peers, cap, share + 128), BF16), shape((n_tok, experts), F32)],
        unit,
        scalar=False,
    )(q, code, gate, mine, b0, d1, d2, e1, e2)
    home = exchange(payload)
    gwg, gwu, gwd, part = call(
        weight_kernel,
        [shape((width, ff), BF16), shape((width, ff), BF16), shape((ff, width), BF16), shape((n_tok, share), F32)],
        12 * unit,
        to_hbm=3,
        raw=range(11),
    )(me, own, pa, pb, na, nb, f0, f1, hid, grads, d_logits, router_t)
    token_grad, router = call(
        functools.partial(home_kernel, cap),
        [shape((n_tok, share), BF16), shape((share // 128, 128), F32)],
        unit,
        to_hbm=2,
        scalar=False,
    )(home, code, part)
    return (token_grad, router.reshape(share, 1), gwg[None], gwu[None], gwd[None])


def solution(mesh):
    in_specs = (
        P("ep", None),
        P("ep", None),
        P("ep", None),
        P(),
        P("ep", None, "tp"),
        P("ep", None, "tp"),
        P("ep", "tp", None),
    )
    out_specs = (
        P("ep", "tp"),
        P("tp", "ep"),
        P("ep", None, "tp"),
        P("ep", None, "tp"),
        P("ep", "tp", None),
    )

    return jax.shard_map(per_device, mesh=mesh, in_specs=in_specs, out_specs=out_specs, check_vma=False)
```

profile of v0, /device:TPU:1, one launch (start us, length us, event | category | flops | bytes accessed | tf_op | source)
XLA Modules:
  0.0 159.5 jit_solution(4002199060572682945)
XLA Ops:
  0.6 2.2 %shard_map.110 = (bf16[512,1024]{1,0:T(8,128)(2,1)S(1)}, f32[48,64]{1,0:T(8,128)S(1)}, f32[48,64]{1,0:T(8,128)S(1)}, bf16[48,512]{1,0:T(8,128)(2,1)S(1)}) custom-call(s32[1]{0:T(128)} %bitcast.tp_ref, bf16[48,2048]{1,0:T(8,128)(2,1)} %tok_ref.1, bf16[48,2048]{1,0:T(8,128)(2,1)} %og_ref.1, s32[4,48]{1,0:T(4,128)} %bitcast.29, bf16[64,2048]{1,0:T(8,128)(2,1)} %bitcast.27), custom_call_target="tpu_custom_call" | custom-call | flops 201326592 | bytes 4194304 | tf_op jit(solution)/shard_map/pallas_call | solution.py:228
  2.8 41.1 %all_to_all.15 = bf16[64,8,1024]{2,1,0:T(8,128)(2,1)S(1)} all-to-all(bf16[64,8,1024]{2,1,0:T(8,128)(2,1)S(1)} %bitcast.22), channel_id=1, replica_groups=mesh['ep'=64,'tp'=4] {'ep'}, dimensions={0} | all-to-all | bytes 2097152 | tf_op jit(solution)/shard_map/all_to_all | solution.py:262
  44.0 2.6 %collective-permute-start.2 = (bf16[256,1024]{1,0:T(8,128)(2,1)S(1)}, bf16[256,1024]{1,0:T(8,128)(2,1)S(1)}, u32[]{:S(2)}, u32[]{:S(2)}) collective-permute-start(bf16[256,1024]{1,0:T(8,128)(2,1)S(1)} %get-tuple-element.61), channel_id=1, source_target_pairs={{0,3},{1,0},{2,1},{3,2},{4,7},{5,4},{6,5},{7,6},{8,11},{9,8},{10,9... | collective-permute-start | bytes 1572872 | tf_op jit(solution)/shard_map/ppermute | solution.py:259
  46.7 2.5 %collective-permute-start.5 = (bf16[256,1024]{1,0:T(8,128)(2,1)S(1)}, bf16[256,1024]{1,0:T(8,128)(2,1)S(1)}, u32[]{:S(2)}, u32[]{:S(2)}) collective-permute-start(bf16[256,1024]{1,0:T(8,128)(2,1)S(1)} %get-tuple-element.62), channel_id=1, source_target_pairs={{0,3},{1,0},{2,1},{3,2},{4,7},{5,4},{6,5},{7,6},{8,11},{9,8},{10,9... | collective-permute-start | bytes 1572872 | tf_op jit(solution)/shard_map/ppermute | solution.py:259
  49.2 7.4 %collective-permute-done.2.nb = bf16[256,1024]{1,0:T(8,128)(2,1)S(1)} collective-permute-done((bf16[256,1024]{1,0:T(8,128)(2,1)S(1)}, bf16[256,1024]{1,0:T(8,128)(2,1)S(1)}, u32[]{:S(2)}, u32[]{:S(2)}) %collective-permute-start.2) | collective-permute-done | bytes 524320 | tf_op jit(solution)/shard_map/ppermute | solution.py:259
  56.7 3.4 %collective-permute-start.3 = (bf16[256,1024]{1,0:T(8,128)(2,1)S(1)}, bf16[256,1024]{1,0:T(8,128)(2,1)S(1)}, u32[]{:S(2)}, u32[]{:S(2)}) collective-permute-start(bf16[256,1024]{1,0:T(8,128)(2,1)S(1)} %collective-permute-done.2.nb), channel_id=1, source_target_pairs={{0,3},{1,0},{2,1},{3,2},{4,7},{5,4},{6,5},{7,6},{8,11},{9,8},{10,9... | collective-permute-start | bytes 1572872 | tf_op jit(solution)/shard_map/ppermute | solution.py:259
  60.1 2.6 %shard_map.111 = (bf16[2048,768]{1,0:T(8,128)(2,1)S(1)}, bf16[384,2048]{1,0:T(8,128)(2,1)S(1)}) custom-call(bf16[2048,384]{1,0:T(8,128)(2,1)} %bitcast.24, bf16[2048,384]{1,0:T(8,128)(2,1)} %bitcast.25, bf16[384,2048]{1,0:T(8,128)(2,1)} %bitcast.26), custom_call_target="tpu_custom_call" | custom-call | flops 201326592 | bytes 4194304 | tf_op jit(solution)/shard_map/pallas_call | solution.py:287
  62.7 8.4 %collective-permute-done.4.pb = bf16[256,1024]{1,0:T(8,128)(2,1)S(1)} collective-permute-done((bf16[256,1024]{1,0:T(8,128)(2,1)S(1)}, bf16[256,1024]{1,0:T(8,128)(2,1)S(1)}, u32[]{:S(2)}, u32[]{:S(2)}) %collective-permute-start.4) | collective-permute-done | bytes 524320 | tf_op jit(solution)/shard_map/ppermute | solution.py:259
  71.1 2.2 %shard_map.112 = (f32[512,768]{1,0:T(8,128)S(1)}, f32[512,384]{1,0:T(8,128)S(1)}) custom-call(s32[1]{0:T(128)} %bitcast.tp_ref, bf16[512,1024]{1,0:T(8,128)(2,1)S(1)} %bitcast.20, bf16[256,1024]{1,0:T(8,128)(2,1)S(1)} %collective-permute-done.pa, bf16[256,1024]{1,0:T(8,128)(2,1)S(1)} %collective-permute-done.4.pb, ...), custom_call_target="tpu_custom_call" | custom-call | flops 1811939328 | bytes 4194304 | tf_op jit(solution)/shard_map/pallas_call | solution.py:228
  73.3 5.8 %collective-permute-done.3.f1 = bf16[256,1024]{1,0:T(8,128)(2,1)S(1)} collective-permute-done((bf16[256,1024]{1,0:T(8,128)(2,1)S(1)}, bf16[256,1024]{1,0:T(8,128)(2,1)S(1)}, u32[]{:S(2)}, u32[]{:S(2)}) %collective-permute-start.3) | collective-permute-done | bytes 524320 | tf_op jit(solution)/shard_map/ppermute | solution.py:259
  79.2 3.1 %collective-permute-done.1.f0 = bf16[256,1024]{1,0:T(8,128)(2,1)S(1)} collective-permute-done((bf16[256,1024]{1,0:T(8,128)(2,1)S(1)}, bf16[256,1024]{1,0:T(8,128)(2,1)S(1)}, u32[]{:S(2)}, u32[]{:S(2)}) %collective-permute-start.1) | collective-permute-done | bytes 524320 | tf_op jit(solution)/shard_map/ppermute | solution.py:259
  82.3 2.2 %shard_map.113 = (bf16[512,384]{1,0:T(8,128)(2,1)S(1)}, bf16[512,768]{1,0:T(8,128)(2,1)S(1)}, f32[64,128]{1,0:T(8,128)S(1)}, bf16[256,512]{1,0:T(8,128)(2,1)S(1)}, bf16[256,512]{1,0:T(8,128)(2,1)S(1)}) custom-call(s32[1]{0:T(128)} %bitcast.tp_ref, bf16[256,1024]{1,0:T(8,128)(2,1)S(1)} %collective-permute-done.1.f0, ...), custom_call_target="tpu_custom_call" | custom-call | flops 1006632960 | bytes 4194304 | tf_op jit(solution)/shard_map/pallas_call | solution.py:228
  84.6 2.7 %collective-permute-start.12 = (bf16[256,512]{1,0:T(8,128)(2,1)S(1)}, bf16[256,512]{1,0:T(8,128)(2,1)S(1)}, u32[]{:S(2)}, u32[]{:S(2)}) collective-permute-start(bf16[256,512]{1,0:T(8,128)(2,1)S(1)} %get-tuple-element.49), channel_id=1, source_target_pairs={{0,3},{1,0},{2,1},{3,2},{4,7},{5,4},{6,5},{7,6},{8,11},{9,8},{10,9... | collective-permute-start | bytes 786440 | tf_op jit(solution)/shard_map/ppermute | solution.py:259
  88.8 2.7 %collective-permute-start.10 = (bf16[256,512]{1,0:T(8,128)(2,1)S(1)}, bf16[256,512]{1,0:T(8,128)(2,1)S(1)}, u32[]{:S(2)}, u32[]{:S(2)}) collective-permute-start(bf16[256,512]{1,0:T(8,128)(2,1)S(1)} %get-tuple-element.45), channel_id=1, source_target_pairs={{0,3},{1,0},{2,1},{3,2},{4,7},{5,4},{6,5},{7,6},{8,11},{9,8},{10,9... | collective-permute-start | bytes 786440 | tf_op jit(solution)/shard_map/ppermute | solution.py:259
  91.6 2.7 %collective-permute-start.14 = (bf16[256,512]{1,0:T(8,128)(2,1)S(1)}, bf16[256,512]{1,0:T(8,128)(2,1)S(1)}, u32[]{:S(2)}, u32[]{:S(2)}) collective-permute-start(bf16[256,512]{1,0:T(8,128)(2,1)S(1)} %get-tuple-element.51), channel_id=1, source_target_pairs={{0,3},{1,0},{2,1},{3,2},{4,7},{5,4},{6,5},{7,6},{8,11},{9,8},{10,9... | collective-permute-start | bytes 786440 | tf_op jit(solution)/shard_map/ppermute | solution.py:259
  95.0 6.5 %collective-permute-done.8.d = f32[64,128]{1,0:T(8,128)S(1)} collective-permute-done((f32[64,128]{1,0:T(8,128)S(1)}, f32[64,128]{1,0:T(8,128)S(1)}, u32[]{:S(2)}, u32[]{:S(2)}) %collective-permute-start.8) | collective-permute-done | bytes 32800 | tf_op jit(solution)/shard_map/ppermute | solution.py:259
  101.5 4.0 %collective-permute-start.7 = (f32[64,128]{1,0:T(8,128)S(1)}, f32[64,128]{1,0:T(8,128)S(1)}, u32[]{:S(2)}, u32[]{:S(2)}) collective-permute-start(f32[64,128]{1,0:T(8,128)S(1)} %get-tuple-element.38.a), channel_id=1, source_target_pairs={{0,3},{1,0},{2,1},{3,2},{4,7},{5,4},{6,5},{7,6},{8,11},{9,8},{10,9... | collective-permute-start | bytes 98312 | tf_op jit(solution)/shard_map/ppermute | solution.py:259
  106.6 4.2 %collective-permute-done.6.b = f32[64,128]{1,0:T(8,128)S(1)} collective-permute-done((f32[64,128]{1,0:T(8,128)S(1)}, f32[64,128]{1,0:T(8,128)S(1)}, u32[]{:S(2)}, u32[]{:S(2)}) %collective-permute-start.6) | collective-permute-done | bytes 32800 | tf_op jit(solution)/shard_map/ppermute | solution.py:259
  111.4 10.7 %all-to-all-start.1 = ((f32[64,1,128]{2,1,0:T(1,128)}), f32[64,1,128]{2,1,0:T(1,128)S(1)}, u32[]{:S(2)}, u32[]{:S(2)}) async-start(f32[64,1,128]{2,1,0:T(1,128)} %bitcast.11), calls=%async_computation.1 | async-start | bytes 65536 | tf_op jit(solution)/shard_map/all_to_all | solution.py:262
  122.1 9.3 %all-to-all-done.1 = f32[64,1,128]{2,1,0:T(1,128)S(1)} async-done(((f32[64,1,128]{2,1,0:T(1,128)}), f32[64,1,128]{2,1,0:T(1,128)S(1)}, u32[]{:S(2)}, u32[]{:S(2)}) %all-to-all-start.1) | async-done | bytes 32800 | tf_op jit(solution)/shard_map/all_to_all | solution.py:262
  131.4 1.9 %shard_map.118 = (bf16[64,8,640]{2,1,0:T(8,128)(2,1)}, f32[48,64]{1,0:T(8,128)S(1)}) custom-call(f32[64,128]{1,0:T(8,128)S(1)} %bitcast.23, f32[48,64]{1,0:T(8,128)S(1)} %get-tuple-element.39.code_ref, f32[48,64]{1,0:T(8,128)S(1)} %shard_map.115.gate_ref, bf16[48,512]{1,0:T(8,128)(2,1)S(1)} %get-tuple-element.41.tok_ref, ...), custom_call_target="tpu_custom_call" | custom-call | flops 201326592 | bytes 4194304 | tf_op jit(solution)/shard_map/pallas_call | solution.py:228
  133.3 4.7 %all-to-all-start.2 = ((bf16[64,8,640]{2,1,0:T(8,128)(2,1)}), bf16[64,8,640]{2,1,0:T(8,128)(2,1)S(1)}, u32[]{:S(2)}, u32[]{:S(2)}) async-start(bf16[64,8,640]{2,1,0:T(8,128)(2,1)} %get-tuple-element.52), calls=%async_computation.2 | async-start | bytes 1310720 | tf_op jit(solution)/shard_map/all_to_all | solution.py:262
  138.1 7.3 %shard_map.119 = (bf16[2048,384]{1,0:T(8,128)(2,1)}, bf16[2048,384]{1,0:T(8,128)(2,1)}, bf16[384,2048]{1,0:T(8,128)(2,1)}, f32[48,512]{1,0:T(8,128)S(1)}) custom-call(s32[1]{0:T(128)} %bitcast.tp_ref, bf16[512,1024]{1,0:T(8,128)(2,1)} %bitcast.21, bf16[256,1024]{1,0:T(8,128)(2,1)} %copy-done.2, bf16[256,1024]{1,0:T(8,128)(2,1)} %copy-done.3, ...), custom_call_target="tpu_custom_call" | custom-call | flops 2415919104 | bytes 4194304 | tf_op jit(solution)/shard_map/pallas_call | solution.py:228
  145.4 13.2 %all-to-all-done.2.home_ref = bf16[64,8,640]{2,1,0:T(8,128)(2,1)S(1)} async-done(((bf16[64,8,640]{2,1,0:T(8,128)(2,1)}), bf16[64,8,640]{2,1,0:T(8,128)(2,1)S(1)}, u32[]{:S(2)}, u32[]{:S(2)}) %all-to-all-start.2) | async-done | bytes 655392 | tf_op jit(solution)/shard_map/all_to_all | solution.py:262
  (43 shorter events, 5.5 us)
Async XLA Ops:
  43.9 27.1 %copy-start = (bf16[64,8,1024]{2,1,0:T(8,128)(2,1)}, bf16[64,8,1024]{2,1,0:T(8,128)(2,1)S(1)}, u32[]{:S(2)}) copy-start(bf16[64,8,1024]{2,1,0:T(8,128)(2,1)S(1)} %all_to_all.15) | copy-start | bytes 3145732
  44.0 12.7 %collective-permute-start.2 = (bf16[256,1024]{1,0:T(8,128)(2,1)S(1)}, bf16[256,1024]{1,0:T(8,128)(2,1)S(1)}, u32[]{:S(2)}, u32[]{:S(2)}) collective-permute-start(bf16[256,1024]{1,0:T(8,128)(2,1)S(1)} %get-tuple-element.61), channel_id=1, source_target_pairs={{0,3},{1,0},{2,1},{3,2},{4,7},{5,4},{6,5},{7,6},{8,11},{9,8},{10,9... | collective-permute-start | bytes 1572872 | tf_op jit(solution)/shard_map/ppermute | solution.py:259
  46.5 13.5 %collective-permute-start = (bf16[256,1024]{1,0:T(8,128)(2,1)S(1)}, bf16[256,1024]{1,0:T(8,128)(2,1)S(1)}, u32[]{:S(2)}, u32[]{:S(2)}) collective-permute-start(bf16[256,1024]{1,0:T(8,128)(2,1)S(1)} %get-tuple-element.62), channel_id=1, source_target_pairs={{0,1},{1,2},{2,3},{3,0},{4,5},{5,6},{6,7},{7,4},{8,9},{9,10},{10,1... | collective-permute-start | bytes 1572872 | tf_op jit(solution)/shard_map/ppermute | solution.py:259
  46.5 24.5 %collective-permute-start.4 = (bf16[256,1024]{1,0:T(8,128)(2,1)S(1)}, bf16[256,1024]{1,0:T(8,128)(2,1)S(1)}, u32[]{:S(2)}, u32[]{:S(2)}) collective-permute-start(bf16[256,1024]{1,0:T(8,128)(2,1)S(1)} %get-tuple-element.61), channel_id=1, source_target_pairs={{0,1},{1,2},{2,3},{3,0},{4,5},{5,6},{6,7},{7,4},{8,9},{9,10},{10,1... | collective-permute-start | bytes 1572872 | tf_op jit(solution)/shard_map/ppermute | solution.py:259
  46.7 24.3 %collective-permute-start.5 = (bf16[256,1024]{1,0:T(8,128)(2,1)S(1)}, bf16[256,1024]{1,0:T(8,128)(2,1)S(1)}, u32[]{:S(2)}, u32[]{:S(2)}) collective-permute-start(bf16[256,1024]{1,0:T(8,128)(2,1)S(1)} %get-tuple-element.62), channel_id=1, source_target_pairs={{0,3},{1,0},{2,1},{3,2},{4,7},{5,4},{6,5},{7,6},{8,11},{9,8},{10,9... | collective-permute-start | bytes 1572872 | tf_op jit(solution)/shard_map/ppermute | solution.py:259
  56.7 14.4 %copy-start.1 = (bf16[256,1024]{1,0:T(8,128)(2,1)}, bf16[256,1024]{1,0:T(8,128)(2,1)S(1)}, u32[]{:S(2)}) copy-start(bf16[256,1024]{1,0:T(8,128)(2,1)S(1)} %collective-permute-done.2.nb) | copy-start | bytes 1572868
  56.7 22.5 %collective-permute-start.3 = (bf16[256,1024]{1,0:T(8,128)(2,1)S(1)}, bf16[256,1024]{1,0:T(8,128)(2,1)S(1)}, u32[]{:S(2)}, u32[]{:S(2)}) collective-permute-start(bf16[256,1024]{1,0:T(8,128)(2,1)S(1)} %collective-permute-done.2.nb), channel_id=1, source_target_pairs={{0,3},{1,0},{2,1},{3,2},{4,7},{5,4},{6,5},{7,6},{8,11},{9,8},{10,9... | collective-permute-start | bytes 1572872 | tf_op jit(solution)/shard_map/ppermute | solution.py:259
  60.1 11.0 %copy-start.2 = (bf16[256,1024]{1,0:T(8,128)(2,1)}, bf16[256,1024]{1,0:T(8,128)(2,1)S(1)}, u32[]{:S(2)}) copy-start(bf16[256,1024]{1,0:T(8,128)(2,1)S(1)} %collective-permute-done.pa) | copy-start | bytes 1572868
  60.1 22.2 %collective-permute-start.1 = (bf16[256,1024]{1,0:T(8,128)(2,1)S(1)}, bf16[256,1024]{1,0:T(8,128)(2,1)S(1)}, u32[]{:S(2)}, u32[]{:S(2)}) collective-permute-start(bf16[256,1024]{1,0:T(8,128)(2,1)S(1)} %collective-permute-done.pa), channel_id=1, source_target_pairs={{0,1},{1,2},{2,3},{3,0},{4,5},{5,6},{6,7},{7,4},{8,9},{9,10},{10,1... | collective-permute-start | bytes 1572872 | tf_op jit(solution)/shard_map/ppermute | solution.py:259
  79.1 5.3 %copy-start.5 = (bf16[256,1024]{1,0:T(8,128)(2,1)}, bf16[256,1024]{1,0:T(8,128)(2,1)S(1)}, u32[]{:S(2)}) copy-start(bf16[256,1024]{1,0:T(8,128)(2,1)S(1)} %collective-permute-done.3.f1) | copy-start | bytes 1572868
  84.5 4.2 %copy-start.7 = (bf16[512,768]{1,0:T(8,128)(2,1)}, bf16[512,768]{1,0:T(8,128)(2,1)S(1)}, u32[]{:S(2)}) copy-start(bf16[512,768]{1,0:T(8,128)(2,1)S(1)} %get-tuple-element.42.grads_ref.grads) | copy-start | bytes 2359300
  84.5 4.2 %copy-start.8 = (bf16[512,384]{1,0:T(8,128)(2,1)}, bf16[512,384]{1,0:T(8,128)(2,1)S(1)}, u32[]{:S(2)}) copy-start(bf16[512,384]{1,0:T(8,128)(2,1)S(1)} %get-tuple-element.53.hid) | copy-start | bytes 1179652
  84.5 7.0 %collective-permute-start.11 = (bf16[256,512]{1,0:T(8,128)(2,1)S(1)}, bf16[256,512]{1,0:T(8,128)(2,1)S(1)}, u32[]{:S(2)}, u32[]{:S(2)}) collective-permute-start(bf16[256,512]{1,0:T(8,128)(2,1)S(1)} %get-tuple-element.47), channel_id=1, source_target_pairs={{0,1},{1,2},{2,3},{3,0},{4,5},{5,6},{6,7},{7,4},{8,9},{9,10},{10,1... | collective-permute-start | bytes 786440 | tf_op jit(solution)/shard_map/ppermute | solution.py:259
  84.6 6.9 %collective-permute-start.12 = (bf16[256,512]{1,0:T(8,128)(2,1)S(1)}, bf16[256,512]{1,0:T(8,128)(2,1)S(1)}, u32[]{:S(2)}, u32[]{:S(2)}) collective-permute-start(bf16[256,512]{1,0:T(8,128)(2,1)S(1)} %get-tuple-element.49), channel_id=1, source_target_pairs={{0,3},{1,0},{2,1},{3,2},{4,7},{5,4},{6,5},{7,6},{8,11},{9,8},{10,9... | collective-permute-start | bytes 786440 | tf_op jit(solution)/shard_map/ppermute | solution.py:259
  88.7 42.7 %collective-permute-start.9 = (bf16[256,512]{1,0:T(8,128)(2,1)}, bf16[256,512]{1,0:T(8,128)(2,1)S(1)}, u32[]{:S(2)}, u32[]{:S(2)}) collective-permute-start(bf16[256,512]{1,0:T(8,128)(2,1)} %get-tuple-element.44), channel_id=1, source_target_pairs={{0,1},{1,2},{2,3},{3,0},{4,5},{5,6},{6,7},{7,4},{8,9},{9,10},{10,1... | collective-permute-start | bytes 786440 | tf_op jit(solution)/shard_map/ppermute | solution.py:259
  88.8 42.6 %collective-permute-start.10 = (bf16[256,512]{1,0:T(8,128)(2,1)S(1)}, bf16[256,512]{1,0:T(8,128)(2,1)S(1)}, u32[]{:S(2)}, u32[]{:S(2)}) collective-permute-start(bf16[256,512]{1,0:T(8,128)(2,1)S(1)} %get-tuple-element.45), channel_id=1, source_target_pairs={{0,3},{1,0},{2,1},{3,2},{4,7},{5,4},{6,5},{7,6},{8,11},{9,8},{10,9... | collective-permute-start | bytes 786440 | tf_op jit(solution)/shard_map/ppermute | solution.py:259
  91.5 39.9 %collective-permute-start.13 = (bf16[256,512]{1,0:T(8,128)(2,1)S(1)}, bf16[256,512]{1,0:T(8,128)(2,1)S(1)}, u32[]{:S(2)}, u32[]{:S(2)}) collective-permute-start(bf16[256,512]{1,0:T(8,128)(2,1)S(1)} %get-tuple-element.50), channel_id=1, source_target_pairs={{0,1},{1,2},{2,3},{3,0},{4,5},{5,6},{6,7},{7,4},{8,9},{9,10},{10,1... | collective-permute-start | bytes 786440 | tf_op jit(solution)/shard_map/ppermute | solution.py:259
  91.6 39.8 %collective-permute-start.14 = (bf16[256,512]{1,0:T(8,128)(2,1)S(1)}, bf16[256,512]{1,0:T(8,128)(2,1)S(1)}, u32[]{:S(2)}, u32[]{:S(2)}) collective-permute-start(bf16[256,512]{1,0:T(8,128)(2,1)S(1)} %get-tuple-element.51), channel_id=1, source_target_pairs={{0,3},{1,0},{2,1},{3,2},{4,7},{5,4},{6,5},{7,6},{8,11},{9,8},{10,9... | collective-permute-start | bytes 786440 | tf_op jit(solution)/shard_map/ppermute | solution.py:259
  94.3 7.2 %collective-permute-start.8 = (f32[64,128]{1,0:T(8,128)S(1)}, f32[64,128]{1,0:T(8,128)S(1)}, u32[]{:S(2)}, u32[]{:S(2)}) collective-permute-start(f32[64,128]{1,0:T(8,128)S(1)} %get-tuple-element.38.a), channel_id=1, source_target_pairs={{0,2},{1,3},{2,0},{3,1},{4,6},{5,7},{6,4},{7,5},{8,10},{9,11},{10,... | collective-permute-start | bytes 98312 | tf_op jit(solution)/shard_map/ppermute | solution.py:259
  101.5 5.0 %collective-permute-start.7 = (f32[64,128]{1,0:T(8,128)S(1)}, f32[64,128]{1,0:T(8,128)S(1)}, u32[]{:S(2)}, u32[]{:S(2)}) collective-permute-start(f32[64,128]{1,0:T(8,128)S(1)} %get-tuple-element.38.a), channel_id=1, source_target_pairs={{0,3},{1,0},{2,1},{3,2},{4,7},{5,4},{6,5},{7,6},{8,11},{9,8},{10,9... | collective-permute-start | bytes 98312 | tf_op jit(solution)/shard_map/ppermute | solution.py:259
  106.5 4.3 %collective-permute-start.6 = (f32[64,128]{1,0:T(8,128)S(1)}, f32[64,128]{1,0:T(8,128)S(1)}, u32[]{:S(2)}, u32[]{:S(2)}) collective-permute-start(f32[64,128]{1,0:T(8,128)S(1)} %get-tuple-element.38.a), channel_id=1, source_target_pairs={{0,1},{1,2},{2,3},{3,0},{4,5},{5,6},{6,7},{7,4},{8,9},{9,10},{10,1... | collective-permute-start | bytes 98312 | tf_op jit(solution)/shard_map/ppermute | solution.py:259
  111.4 20.0 %all-to-all-start.1 = ((f32[64,1,128]{2,1,0:T(1,128)}), f32[64,1,128]{2,1,0:T(1,128)S(1)}, u32[]{:S(2)}, u32[]{:S(2)}) async-start(f32[64,1,128]{2,1,0:T(1,128)} %bitcast.11), calls=%async_computation.1 | async-start | bytes 65536 | tf_op jit(solution)/shard_map/all_to_all | solution.py:262
  133.3 4.8 %copy-start.9 = (f32[48,64]{1,0:T(8,128)}, f32[48,64]{1,0:T(8,128)S(1)}, u32[]{:S(2)}) copy-start(f32[48,64]{1,0:T(8,128)S(1)} %get-tuple-element.54.d_logits_ref) | copy-start | bytes 36868
  133.3 25.2 %all-to-all-start.2 = ((bf16[64,8,640]{2,1,0:T(8,128)(2,1)}), bf16[64,8,640]{2,1,0:T(8,128)(2,1)S(1)}, u32[]{:S(2)}, u32[]{:S(2)}) async-start(bf16[64,8,640]{2,1,0:T(8,128)(2,1)} %get-tuple-element.52), calls=%async_computation.2 | async-start | bytes 1310720 | tf_op jit(solution)/shard_map/all_to_all | solution.py:262
  (3 other events, 6.8 us)
where the time goes:
time: 160 us
  waiting for transfers between devices  58.9 us (37%)
  blocking collectives  41.1 us (26%)
  starting transfers between devices  37.2 us (23%)
  Pallas kernels  21.4 us (13%)
    all_to_all x1, blocking collectives, exchange(): return lax.all_to_all(value, 'ep', split_axis=0, concat_axis=0, tiled=True)  41.1 us
    ppermute x15, waiting for transfers between devices, hop(): return lax.ppermute(value, 'tp', [(i, (i + by) % tp) for i in range(tp)])  36.4 us
    all_to_all x2, waiting for transfers between devices, exchange(): return lax.all_to_all(value, 'ep', split_axis=0, concat_axis=0, tiled=True)  22.5 us
    ppermute x15, starting transfers between devices, hop(): return lax.ppermute(value, 'tp', [(i, (i + by) % tp) for i in range(tp)])  21.8 us
    pallas_call x10, Pallas kernels, run(): pl.pallas_call(body, out_shape=outs[:to_hbm] + [pltpu.VMEM(o.shape, o.dty...  18.9 us
    all_to_all x2, starting transfers between devices, exchange(): return lax.all_to_all(value, 'ep', split_axis=0, concat_axis=0, tiled=True)  15.4 us
  transfers between devices with their start and end apart: 17, of which 9 were waited for; matrix products, arithmetic and copies ran while one was open for 0% of the time, Pallas kernels for 9%

commit v1 on v0

--- a/solution.py
+++ b/solution.py
@@ -37,10 +37,10 @@
     return ((iota((rows, experts), 0) >> bits(cap)) == iota((rows, experts), 1)).astype(F32)
 
 
-def dispatch_kernel(cap, tp_ref, tok_ref, og_ref, ids_ref, rw_ref, send_ref, code_ref, gate_ref, mine_ref):
+def dispatch_kernel(cap, tp_ref, tok_ref, og_ref, ids_ref, rw_ref, send_ref, more_ref, code_ref, gate_ref, mine_ref):
     n_tok = tok_ref.shape[0]
     experts = rw_ref.shape[0]
-    share = send_ref.shape[1] // 2
+    share = mine_ref.shape[1]
     start = pl.multiple_of(tp_ref[0] * share, share)
     logits = mm(tok_ref[...], rw_ref[...], NT)
     ids = ids_ref[...].astype(F32).T
@@ -70,17 +70,17 @@
     gate_of = jnp.sum(jnp.where(pick, gate_of, 0.0), axis=1, keepdims=True)
     mine = tok_ref[:, pl.ds(start, share)]
     mine_ref[...] = mine
-    both = mm(pick.astype(F32).astype(BF16), jnp.concatenate([mine, og_ref[:, pl.ds(start, share)]], axis=1), NN)
+    relay = send_ref.shape[1] - share
+    cots = [og_ref[:, pl.ds(start, relay)]]
+    cots += [og_ref[:, j + relay : j + share] for j in range(0, og_ref.shape[1], share)]
+    both = mm(pick.astype(F32).astype(BF16), jnp.concatenate([mine] + cots, axis=1), NN)
     send_ref[:, :share] = both[:, :share].astype(BF16)
-    send_ref[:, share:] = (both[:, share:] * gate_of).astype(BF16)
-
-
-LEFT, RIGHT = 0, 1
-
-
-def joined(refs, side):
-    share = refs[0].shape[1] // 2
-    return jnp.concatenate([r[:, side * share : (side + 1) * share] for r in refs], axis=0)
+    send_ref[:, share:] = (both[:, share : share + relay] * gate_of).astype(BF16)
+    more_ref[...] = (both[:, share + relay :] * gate_of).astype(BF16)
+
+
+def joined(refs, cols):
+    return jnp.concatenate([r[:, cols] for r in refs], axis=0)
 
 
 def block(tp_ref, off, share):
@@ -91,7 +91,11 @@
     total = start
     for off, refs in groups:
         at = block(tp_ref, off, share)
-        terms = (mm(joined(refs, LEFT), wgu[at, :], NN), mm(joined(refs, RIGHT), wd[:, at], NT))
+        relay = refs[0].shape[1] - share
+        terms = (
+            mm(joined(refs, slice(0, share)), wgu[at, :], NN),
+            mm(joined(refs, slice(share, None)), wd[:, pl.ds(at.start, relay)], NT),
+        )
         total = terms if total is None else tuple(a + b for a, b in zip(total, terms))
     return total
 
@@ -115,14 +119,16 @@
     return hidden.astype(BF16), grads, mm(group, spot, NN, HI)
 
 
-def near_kernel(tp_ref, own, pa, pb, na, nb, wgu, wd, pre, bk):
+def near_kernel(share, tp_ref, own, pa, pb, na, nb, more, wgu, wd, pre, bk):
     groups = ((0, (own,)), (3, (pa, pb)), (1, (na, nb)))
-    pre[...], bk[...] = forward(tp_ref, groups, own.shape[1] // 2, wgu, wd)
+    relay = own.shape[1] - share
+    rest = jnp.concatenate([wd[:, j + relay : j + share] for j in range(0, wd.shape[1], share)], axis=1)
+    pre[...], back = forward(tp_ref, groups, share, wgu, wd)
+    bk[...] = back + mm(more[...], rest, NT)
 
 
 def far_kernel(cap, tp_ref, f0, f1, pre, bk, wgu, wd, hid, grads, score, b2a, b2b):
-    share = f0.shape[1] // 2
-    half = f0.shape[0]
+    half, share = b2a.shape
     start = (pre[...], bk[...])
     hid[...], values, score[...] = units(cap, *forward(tp_ref, ((2, (f0, f1)),), share, wgu, wd, start))
     grads[...] = values
@@ -131,7 +137,7 @@
     b2b[...] = far[half:]
 
 
-def token_kernel(tp_ref, grads_ref, wgu, b1a, b1b, b3a, b3b, b0):
+def token_kernel(tp_ref, grads_ref, wgu, b1a, b3b, b0, b1b, b3a):
     share = b0.shape[1]
     half = b0.shape[0] // 2
     grads = grads_ref[...]
@@ -157,18 +163,20 @@
     behind[...] = (b3b[...] + s2[...].astype(F32)).astype(BF16)
 
 
-def weight_kernel(tp_ref, own, pa, pb, na, nb, f0, f1, hid, grads, d_logits_ref, rw_ref,
+def weight_kernel(share, tp_ref, own, pa, pb, na, nb, f0, f1, more, hid, grads, d_logits_ref, rw_ref,
                   gwg_ref, gwu_ref, gwd_ref, part_ref):
-    share = own.shape[1] // 2
     ff = gwg_ref.shape[1]
+    relay = own.shape[1] - share
     part_ref[...] = mm(d_logits_ref[...], rw_ref[:, block(tp_ref, 0, share)].astype(F32), NN, HI)
+    rest = mm(hid[...], more[...], TN).astype(BF16)
+    for j in range(gwd_ref.shape[1] // share):
+        gwd_ref[:, j * share + relay : (j + 1) * share] = rest[:, j * (share - relay) : (j + 1) * (share - relay)]
     for off, refs in ((0, (own,)), (3, (pa, pb)), (1, (na, nb)), (2, (f0, f1))):
         at = block(tp_ref, off, share)
-        t, g = joined(refs, LEFT), joined(refs, RIGHT)
-        both = mm(t, grads[...], TN).astype(BF16)
+        both = mm(joined(refs, slice(0, share)), grads[...], TN).astype(BF16)
         gwg_ref[at, :] = both[:, :ff]
         gwu_ref[at, :] = both[:, ff:]
-        gwd_ref[:, at] = mm(hid[...], g, TN).astype(BF16)
+        gwd_ref[:, pl.ds(at.start, relay)] = mm(hid[...], joined(refs, slice(share, None)), TN).astype(BF16)
 
 
 def router_kernel(cap, q_ref, code_ref, gate_ref, tok_ref, *refs):
@@ -227,7 +235,7 @@
         ins = args[1:] if scalar else args
         return pl.pallas_call(
             body,
-            out_shape=outs[:to_hbm] + [pltpu.VMEM(o.shape, o.dtype) for o in outs[to_hbm:]],
+            out_shape=[(pltpu.HBM if i < to_hbm else pltpu.VMEM)(o.shape, o.dtype) for i, o in enumerate(outs)],
             in_specs=([SMEM] if scalar else []) + [VMEM] * len(ins),
             out_specs=[VMEM] * len(outs),
             cost_estimate=cost(flops, 4 << 20),
@@ -261,14 +269,17 @@
     def exchange(value):
         return lax.all_to_all(value, "ep", split_axis=0, concat_axis=0, tiled=True)
 
-    send, code, gate, mine = call(
+    relay = share - 128
+    rest = tp * (share - relay)
+    send, more, code, gate, mine = call(
         functools.partial(dispatch_kernel, cap),
-        [shape((rows, 2 * share), BF16), shape((n_tok, experts), F32), shape((n_tok, experts), F32),
-         shape((n_tok, share), BF16)],
+        [shape((rows, share + relay), BF16), shape((rows, rest), BF16), shape((n_tok, experts), F32),
+         shape((n_tok, experts), F32), shape((n_tok, share), BF16)],
         unit,
         raw=(0, 1, 2, 3),
     )(me, tokens, out_grad, expert_ids.T, router_t)
-    own = exchange(send.reshape(peers, cap, 2 * share)).reshape(rows, 2 * share)
+    own = exchange(send.reshape(peers, cap, share + relay)).reshape(rows, share + relay)
+    more = exchange(more.reshape(peers, cap, rest)).reshape(rows, rest)
     pa, nb = hop(own[:half], 1), hop(own[half:], -1)
     pb, na = hop(own[half:], 1), hop(own[:half], -1)
     f0, f1 = hop(pa, 1), hop(nb, -1)
@@ -295,8 +306,8 @@
     )(*(pltpu.with_memory_space_constraint(w[0], pltpu.HBM) for w in (w_gate, w_up, w_down)))
 
     near = call(
-        near_kernel, [shape((rows, 2 * ff), F32), shape((rows, ff), F32)], 9 * unit
-    )(me, own, pa, pb, na, nb, wgu, wd)
+        functools.partial(near_kernel, share), [shape((rows, 2 * ff), F32), shape((rows, ff), F32)], 9 * unit
+    )(me, own, pa, pb, na, nb, more, wgu, wd)
     hid, grads, score, b2a, b2b = call(
         functools.partial(far_kernel, cap),
         [shape((rows, ff), BF16), shape((rows, 2 * ff), BF16), shape((peers, 128), F32)]
@@ -304,14 +315,14 @@
         5 * unit,
     )(me, f0, f1, *near, wgu, wd)
     s1, s2 = hop(b2a, 1), hop(b2b, -1)
-    b1a, b1b, b3a, b3b, b0 = call(
+    b1a, b3b, b0, b1b, b3a = call(
         token_kernel,
-        [shape((half, share), F32), shape((half, share), BF16), shape((half, share), BF16),
-         shape((half, share), F32), shape((rows, share), F32)],
+        [shape((half, share), F32)] * 2 + [shape((rows, share), F32)] + [shape((half, share), BF16)] * 2,
         6 * unit,
+        to_hbm=3,
     )(me, grads, wgu)
     d1, d2 = hop(b1b, 1), hop(b3a, -1)
-    ahead, behind = call(onward_kernel, [shape((half, share), BF16)] * 2, 1, scalar=False)(b1a, s1, b3b, s2)
+    ahead, behind = call(onward_kernel, [shape((half, share), BF16)] * 2, 1, scalar=False, raw=(0, 2))(b1a, s1, b3b, s2)
     e1, e2 = hop(ahead, 1), hop(behind, -1)
     (gate,) = call(mark_kernel, [shape((n_tok, experts), F32)], 1, scalar=False)(gate)
     (score,) = call(total_kernel, [shape((peers, 128), F32)], 1, scalar=False)(
@@ -323,15 +334,16 @@
         [shape((peers, cap, share + 128), BF16), shape((n_tok, experts), F32)],
         unit,
         scalar=False,
+        raw=(4,),
     )(q, code, gate, mine, b0, d1, d2, e1, e2)
     home = exchange(payload)
     gwg, gwu, gwd, part = call(
-        weight_kernel,
+        functools.partial(weight_kernel, share),
         [shape((width, ff), BF16), shape((width, ff), BF16), shape((ff, width), BF16), shape((n_tok, share), F32)],
         12 * unit,
         to_hbm=3,
-        raw=range(11),
-    )(me, own, pa, pb, na, nb, f0, f1, hid, grads, d_logits, router_t)
+        raw=range(12),
+    )(me, own, pa, pb, na, nb, f0, f1, more, hid, grads, d_logits, router_t)
     token_grad, router = call(
         functools.partial(home_kernel, cap),
         [shape((n_tok, share), BF16), shape((share // 128, 128), F32)],

time: 160 us -> 169 us (1.056)
  waiting for transfers between devices: 58.9 us -> 47.7 us
  starting transfers between devices: 37.2 us -> 47.5 us
  Pallas kernels: 21.4 us -> 28.7 us
  local copies, waits for them, and re-layouts: 0.11 us -> 5.34 us
  blocking collectives: 41.1 us -> 38.5 us
    ppermute x15, waiting for transfers between devices: 36.4 us -> 25.4 us  [hop(): return lax.ppermute(value, 'tp', [(i, (i + by) % tp) for i in range(tp)])]
    all_to_all x2 -> x3, starting transfers between devices: 15.4 us -> 25.9 us  [exchange(): return lax.all_to_all(value, 'ep', split_axis=0, concat_axis=0, tiled=True)]
    pallas_call x10, Pallas kernels: 18.9 us -> 26.3 us  [run(): pl.pallas_call(body, out_shape=[(pltpu.HBM if i < to_hbm else pltpu.VMEM)...]
    unnamed x20 -> x14, local copies, waits for them, and re-layouts: 0.04 us -> 4.34 us
    all_to_all x1, blocking collectives: 41.1 us -> 38.5 us  [exchange(): return lax.all_to_all(value, 'ep', split_axis=0, concat_axis=0, tiled=True)]
    all_to_all x2 -> x3, waiting for transfers between devices: 22.5 us -> 22.3 us  [exchange(): return lax.all_to_all(value, 'ep', split_axis=0, concat_axis=0, tiled=True)]
  transfers between devices with their start and end apart: 17 -> 18, of which waited for: 9 -> 9; matrix products, arithmetic and copies ran while one was open for 0% -> 1% of each run, Pallas kernels for 9% -> 11%
where the time goes in v1:
time: 169 us; the launch traced here: 168 us
  waiting for transfers between devices  47.7 us (28%)
  starting transfers between devices  47.5 us (28%)
  blocking collectives  38.5 us (23%)
  Pallas kernels  28.7 us (17%)
  local copies, waits for them, and re-layouts  5.34 us (3%)
    all_to_all x1, blocking collectives, exchange(): return lax.all_to_all(value, 'ep', split_axis=0, concat_axis=0, tiled=True)  38.5 us
    pallas_call x10, Pallas kernels, run(): pl.pallas_call(body, out_shape=[(pltpu.HBM if i < to_hbm else pltpu.VMEM)...  26.3 us
    all_to_all x3, starting transfers between devices, exchange(): return lax.all_to_all(value, 'ep', split_axis=0, concat_axis=0, tiled=True)  25.9 us
    ppermute x15, waiting for transfers between devices, hop(): return lax.ppermute(value, 'tp', [(i, (i + by) % tp) for i in range(tp)])  25.4 us
    all_to_all x3, waiting for transfers between devices, exchange(): return lax.all_to_all(value, 'ep', split_axis=0, concat_axis=0, tiled=True)  22.3 us
    ppermute x15, starting transfers between devices, hop(): return lax.ppermute(value, 'tp', [(i, (i + by) % tp) for i in range(tp)])  21.6 us
    unnamed x14, local copies, waits for them, and re-layouts  4.34 us
  transfers between devices with their start and end apart: 18, of which 9 were waited for; matrix products, arithmetic and copies ran while one was open for 1% of the time, Pallas kernels for 11%

profile of v1, /device:TPU:1, one launch (start us, length us, event | category | flops | bytes accessed | tf_op | source)
XLA Modules:
  0.0 168.5 jit_solution(7088258320455229813)
XLA Ops:
  0.6 3.1 %shard_map.110 = (bf16[512,896]{1,0:T(8,128)(2,1)S(1)}, bf16[512,512]{1,0:T(8,128)(2,1)}, f32[48,64]{1,0:T(8,128)S(1)}, f32[48,64]{1,0:T(8,128)S(1)}, bf16[48,512]{1,0:T(8,128)(2,1)S(1)}) custom-call(s32[1]{0:T(128)} %bitcast.tp_ref, bf16[48,2048]{1,0:T(8,128)(2,1)} %tok_ref.1, bf16[48,2048]{1,0:T(8,128)(2,1)} %og_ref.1, s32[4,48]{1,0:T(4,128)} %bitcast.31, ...), custom_call_target="tpu_custom_call" | custom-call | flops 201326592 | bytes 4194304 | tf_op jit(solution)/shard_map/pallas_call | solution.py:236
  3.7 38.5 %all_to_all.20 = bf16[64,8,896]{2,1,0:T(8,128)(2,1)S(1)} all-to-all(bf16[64,8,896]{2,1,0:T(8,128)(2,1)S(1)} %bitcast.24), channel_id=1, replica_groups=mesh['ep'=64,'tp'=4] {'ep'}, dimensions={0} | all-to-all | bytes 1835008 | tf_op jit(solution)/shard_map/all_to_all | solution.py:270
  42.2 6.3 %all-to-all-start.1 = ((bf16[64,8,512]{2,1,0:T(8,128)(2,1)}), bf16[64,8,512]{2,1,0:T(8,128)(2,1)}, u32[]{:S(2)}, u32[]{:S(2)}) async-start(bf16[64,8,512]{2,1,0:T(8,128)(2,1)} %bitcast.7), calls=%async_computation.1 | async-start | bytes 1048576 | tf_op jit(solution)/shard_map/all_to_all | solution.py:270
  49.5 2.5 %collective-permute-start.2 = (bf16[256,896]{1,0:T(8,128)(2,1)}, bf16[256,896]{1,0:T(8,128)(2,1)}, u32[]{:S(2)}, u32[]{:S(2)}) collective-permute-start(bf16[256,896]{1,0:T(8,128)(2,1)} %get-tuple-element.63), channel_id=1, source_target_pairs={{0,3},{1,0},{2,1},{3,2},{4,7},{5,4},{6,5},{7,6},{8,11},{9,8},{10,9... | collective-permute-start | bytes 1376264 | tf_op jit(solution)/shard_map/ppermute | solution.py:267
  52.2 2.5 %collective-permute-start.5 = (bf16[256,896]{1,0:T(8,128)(2,1)}, bf16[256,896]{1,0:T(8,128)(2,1)}, u32[]{:S(2)}, u32[]{:S(2)}) collective-permute-start(bf16[256,896]{1,0:T(8,128)(2,1)} %get-tuple-element.64), channel_id=1, source_target_pairs={{0,3},{1,0},{2,1},{3,2},{4,7},{5,4},{6,5},{7,6},{8,11},{9,8},{10,9... | collective-permute-start | bytes 1376264 | tf_op jit(solution)/shard_map/ppermute | solution.py:267
  54.7 7.0 %collective-permute-done.2.nb = bf16[256,896]{1,0:T(8,128)(2,1)} collective-permute-done((bf16[256,896]{1,0:T(8,128)(2,1)}, bf16[256,896]{1,0:T(8,128)(2,1)}, u32[]{:S(2)}, u32[]{:S(2)}) %collective-permute-start.2) | collective-permute-done | bytes 458784 | tf_op jit(solution)/shard_map/ppermute | solution.py:267
  61.6 3.4 %collective-permute-start.3 = (bf16[256,896]{1,0:T(8,128)(2,1)}, bf16[256,896]{1,0:T(8,128)(2,1)}, u32[]{:S(2)}, u32[]{:S(2)}) collective-permute-start(bf16[256,896]{1,0:T(8,128)(2,1)} %collective-permute-done.2.nb), channel_id=1, source_target_pairs={{0,3},{1,0},{2,1},{3,2},{4,7},{5,4},{6,5},{7,6},{8,11},{9,8},{10,9... | collective-permute-start | bytes 1376264 | tf_op jit(solution)/shard_map/ppermute | solution.py:267
  68.6 6.0 %collective-permute-done.4.pb = bf16[256,896]{1,0:T(8,128)(2,1)} collective-permute-done((bf16[256,896]{1,0:T(8,128)(2,1)}, bf16[256,896]{1,0:T(8,128)(2,1)}, u32[]{:S(2)}, u32[]{:S(2)}) %collective-permute-start.4) | collective-permute-done | bytes 458784 | tf_op jit(solution)/shard_map/ppermute | solution.py:267
  77.2 4.0 %shard_map.112 = (f32[512,768]{1,0:T(8,128)S(1)}, f32[512,384]{1,0:T(8,128)S(1)}) custom-call(s32[1]{0:T(128)} %bitcast.tp_ref, bf16[512,896]{1,0:T(8,128)(2,1)S(1)} %bitcast.23, bf16[256,896]{1,0:T(8,128)(2,1)} %collective-permute-done.pa, bf16[256,896]{1,0:T(8,128)(2,1)} %collective-permute-done.4.pb, bf16[256,896]{1,0:T(8,128)(2,1)} %collective-permute-done.5.na, ...), custom_call_target="tpu_custom_call" | custom-call | flops 1811939328 | bytes 4194304 | tf_op jit(solution)/shard_map/pallas_call | solution.py:236
  81.3 3.1 %collective-permute-done.1.f0 = bf16[256,896]{1,0:T(8,128)(2,1)} collective-permute-done((bf16[256,896]{1,0:T(8,128)(2,1)}, bf16[256,896]{1,0:T(8,128)(2,1)}, u32[]{:S(2)}, u32[]{:S(2)}) %collective-permute-start.1) | collective-permute-done | bytes 458784 | tf_op jit(solution)/shard_map/ppermute | solution.py:267
  84.4 3.3 %shard_map.113 = (bf16[512,384]{1,0:T(8,128)(2,1)S(1)}, bf16[512,768]{1,0:T(8,128)(2,1)S(1)}, f32[64,128]{1,0:T(8,128)S(1)}, bf16[256,512]{1,0:T(8,128)(2,1)S(1)}, bf16[256,512]{1,0:T(8,128)(2,1)S(1)}) custom-call(s32[1]{0:T(128)} %bitcast.tp_ref, bf16[256,896]{1,0:T(8,128)(2,1)} %collective-permute-done.1.f0, bf16[256,896]{1,0:T(8,128)(2,1)} %collective-permute-done.3.f1, ...), custom_call_target="tpu_custom_call" | custom-call | flops 1006632960 | bytes 4194304 | tf_op jit(solution)/shard_map/pallas_call | solution.py:236
  88.0 2.7 %collective-permute-start.12 = (bf16[256,512]{1,0:T(8,128)(2,1)S(1)}, bf16[256,512]{1,0:T(8,128)(2,1)S(1)}, u32[]{:S(2)}, u32[]{:S(2)}) collective-permute-start(bf16[256,512]{1,0:T(8,128)(2,1)S(1)} %get-tuple-element.51), channel_id=1, source_target_pairs={{0,3},{1,0},{2,1},{3,2},{4,7},{5,4},{6,5},{7,6},{8,11},{9,8},{10,9... | collective-permute-start | bytes 786440 | tf_op jit(solution)/shard_map/ppermute | solution.py:267
  90.7 2.5 %shard_map.116 = (f32[256,512]{1,0:T(8,128)}, f32[256,512]{1,0:T(8,128)}, f32[512,512]{1,0:T(8,128)}, bf16[256,512]{1,0:T(8,128)(2,1)}, bf16[256,512]{1,0:T(8,128)(2,1)S(1)}) custom-call(s32[1]{0:T(128)} %bitcast.tp_ref, bf16[512,768]{1,0:T(8,128)(2,1)S(1)} %get-tuple-element.44.grads_ref.grads, bf16[2048,768]{1,0:T(8,128)(2,1)S(1)} %get-tuple-element.36.wgu), custom_call_target="tpu_custom_call" | custom-call | flops 1207959552 | bytes 4194304 | tf_op jit(solution)/shard_map/pallas_call | solution.py:236
  93.2 2.7 %collective-permute-start.10 = (bf16[256,512]{1,0:T(8,128)(2,1)S(1)}, bf16[256,512]{1,0:T(8,128)(2,1)S(1)}, u32[]{:S(2)}, u32[]{:S(2)}) collective-permute-start(bf16[256,512]{1,0:T(8,128)(2,1)S(1)} %get-tuple-element.47), channel_id=1, source_target_pairs={{0,3},{1,0},{2,1},{3,2},{4,7},{5,4},{6,5},{7,6},{8,11},{9,8},{10,9... | collective-permute-start | bytes 786440 | tf_op jit(solution)/shard_map/ppermute | solution.py:267
  97.2 2.7 %collective-permute-start.14 = (bf16[256,512]{1,0:T(8,128)(2,1)S(1)}, bf16[256,512]{1,0:T(8,128)(2,1)S(1)}, u32[]{:S(2)}, u32[]{:S(2)}) collective-permute-start(bf16[256,512]{1,0:T(8,128)(2,1)S(1)} %get-tuple-element.53), channel_id=1, source_target_pairs={{0,3},{1,0},{2,1},{3,2},{4,7},{5,4},{6,5},{7,6},{8,11},{9,8},{10,9... | collective-permute-start | bytes 786440 | tf_op jit(solution)/shard_map/ppermute | solution.py:267
  100.3 4.6 %collective-permute-done.8.d = f32[64,128]{1,0:T(8,128)S(1)} collective-permute-done((f32[64,128]{1,0:T(8,128)S(1)}, f32[64,128]{1,0:T(8,128)S(1)}, u32[]{:S(2)}, u32[]{:S(2)}) %collective-permute-start.8) | collective-permute-done | bytes 32800 | tf_op jit(solution)/shard_map/ppermute | solution.py:267
  104.9 3.5 %collective-permute-start.7 = (f32[64,128]{1,0:T(8,128)S(1)}, f32[64,128]{1,0:T(8,128)S(1)}, u32[]{:S(2)}, u32[]{:S(2)}) collective-permute-start(f32[64,128]{1,0:T(8,128)S(1)} %get-tuple-element.40.a), channel_id=1, source_target_pairs={{0,3},{1,0},{2,1},{3,2},{4,7},{5,4},{6,5},{7,6},{8,11},{9,8},{10,9... | collective-permute-start | bytes 98312 | tf_op jit(solution)/shard_map/ppermute | solution.py:267
  110.1 3.6 %collective-permute-done.6.b = f32[64,128]{1,0:T(8,128)S(1)} collective-permute-done((f32[64,128]{1,0:T(8,128)S(1)}, f32[64,128]{1,0:T(8,128)S(1)}, u32[]{:S(2)}, u32[]{:S(2)}) %collective-permute-start.6) | collective-permute-done | bytes 32800 | tf_op jit(solution)/shard_map/ppermute | solution.py:267
  114.3 14.9 %all-to-all-start.2 = ((f32[64,1,128]{2,1,0:T(1,128)}), f32[64,1,128]{2,1,0:T(1,128)S(1)}, u32[]{:S(2)}, u32[]{:S(2)}) async-start(f32[64,1,128]{2,1,0:T(1,128)} %bitcast.13), calls=%async_computation.2 | async-start | bytes 65536 | tf_op jit(solution)/shard_map/all_to_all | solution.py:270
  129.2 9.3 %all-to-all-done.2 = f32[64,1,128]{2,1,0:T(1,128)S(1)} async-done(((f32[64,1,128]{2,1,0:T(1,128)}), f32[64,1,128]{2,1,0:T(1,128)S(1)}, u32[]{:S(2)}, u32[]{:S(2)}) %all-to-all-start.2) | async-done | bytes 32800 | tf_op jit(solution)/shard_map/all_to_all | solution.py:270
  138.6 3.1 %shard_map.118 = (bf16[64,8,640]{2,1,0:T(8,128)(2,1)}, f32[48,64]{1,0:T(8,128)S(1)}) custom-call(f32[64,128]{1,0:T(8,128)S(1)} %bitcast.25, f32[48,64]{1,0:T(8,128)S(1)} %get-tuple-element.41.code_ref, f32[48,64]{1,0:T(8,128)S(1)} %shard_map.115.gate_ref, bf16[48,512]{1,0:T(8,128)(2,1)S(1)} %get-tuple-element.43.tok_ref, ...), custom_call_target="tpu_custom_call" | custom-call | flops 201326592 | bytes 4194304 | tf_op jit(solution)/shard_map/pallas_call | solution.py:236
  142.3 4.8 %all-to-all-start.3 = ((bf16[64,8,640]{2,1,0:T(8,128)(2,1)}), bf16[64,8,640]{2,1,0:T(8,128)(2,1)S(1)}, u32[]{:S(2)}, u32[]{:S(2)}) async-start(bf16[64,8,640]{2,1,0:T(8,128)(2,1)} %get-tuple-element.54), calls=%async_computation.3 | async-start | bytes 1310720 | tf_op jit(solution)/shard_map/all_to_all | solution.py:270
  147.0 7.5 %shard_map.119 = (bf16[2048,384]{1,0:T(8,128)(2,1)}, bf16[2048,384]{1,0:T(8,128)(2,1)}, bf16[384,2048]{1,0:T(8,128)(2,1)}, f32[48,512]{1,0:T(8,128)S(1)}) custom-call(s32[1]{0:T(128)} %bitcast.tp_ref, bf16[512,896]{1,0:T(8,128)(2,1)} %bitcast.22, bf16[256,896]{1,0:T(8,128)(2,1)} %collective-permute-done.pa, bf16[256,896]{1,0:T(8,128)(2,1)} %collective-permute-done.4.pb, ...), custom_call_target="tpu_custom_call" | custom-call | flops 2415919104 | bytes 4194304 | tf_op jit(solution)/shard_map/pallas_call | solution.py:236
  154.6 13.0 %all-to-all-done.3.home_ref = bf16[64,8,640]{2,1,0:T(8,128)(2,1)S(1)} async-done(((bf16[64,8,640]{2,1,0:T(8,128)(2,1)}), bf16[64,8,640]{2,1,0:T(8,128)(2,1)S(1)}, u32[]{:S(2)}, u32[]{:S(2)}) %all-to-all-start.3) | async-done | bytes 655392 | tf_op jit(solution)/shard_map/all_to_all | solution.py:270
  (39 shorter events, 13.4 us)
Async XLA Ops:
  42.2 22.8 %copy-start = (bf16[64,8,896]{2,1,0:T(8,128)(2,1)}, bf16[64,8,896]{2,1,0:T(8,128)(2,1)S(1)}, u32[]{:S(2)}) copy-start(bf16[64,8,896]{2,1,0:T(8,128)(2,1)S(1)} %all_to_all.20) | copy-start | bytes 2752516
  42.2 26.4 %all-to-all-start.1 = ((bf16[64,8,512]{2,1,0:T(8,128)(2,1)}), bf16[64,8,512]{2,1,0:T(8,128)(2,1)}, u32[]{:S(2)}, u32[]{:S(2)}) async-start(bf16[64,8,512]{2,1,0:T(8,128)(2,1)} %bitcast.7), calls=%async_computation.1 | async-start | bytes 1048576 | tf_op jit(solution)/shard_map/all_to_all | solution.py:270
  49.5 12.1 %collective-permute-start.2 = (bf16[256,896]{1,0:T(8,128)(2,1)}, bf16[256,896]{1,0:T(8,128)(2,1)}, u32[]{:S(2)}, u32[]{:S(2)}) collective-permute-start(bf16[256,896]{1,0:T(8,128)(2,1)} %get-tuple-element.63), channel_id=1, source_target_pairs={{0,3},{1,0},{2,1},{3,2},{4,7},{5,4},{6,5},{7,6},{8,11},{9,8},{10,9... | collective-permute-start | bytes 1376264 | tf_op jit(solution)/shard_map/ppermute | solution.py:267
  52.0 13.1 %collective-permute-start = (bf16[256,896]{1,0:T(8,128)(2,1)}, bf16[256,896]{1,0:T(8,128)(2,1)}, u32[]{:S(2)}, u32[]{:S(2)}) collective-permute-start(bf16[256,896]{1,0:T(8,128)(2,1)} %get-tuple-element.64), channel_id=1, source_target_pairs={{0,1},{1,2},{2,3},{3,0},{4,5},{5,6},{6,7},{7,4},{8,9},{9,10},{10,1... | collective-permute-start | bytes 1376264 | tf_op jit(solution)/shard_map/ppermute | solution.py:267
  52.0 22.6 %collective-permute-start.4 = (bf16[256,896]{1,0:T(8,128)(2,1)}, bf16[256,896]{1,0:T(8,128)(2,1)}, u32[]{:S(2)}, u32[]{:S(2)}) collective-permute-start(bf16[256,896]{1,0:T(8,128)(2,1)} %get-tuple-element.63), channel_id=1, source_target_pairs={{0,1},{1,2},{2,3},{3,0},{4,5},{5,6},{6,7},{7,4},{8,9},{9,10},{10,1... | collective-permute-start | bytes 1376264 | tf_op jit(solution)/shard_map/ppermute | solution.py:267
  52.2 22.4 %collective-permute-start.5 = (bf16[256,896]{1,0:T(8,128)(2,1)}, bf16[256,896]{1,0:T(8,128)(2,1)}, u32[]{:S(2)}, u32[]{:S(2)}) collective-permute-start(bf16[256,896]{1,0:T(8,128)(2,1)} %get-tuple-element.64), channel_id=1, source_target_pairs={{0,3},{1,0},{2,1},{3,2},{4,7},{5,4},{6,5},{7,6},{8,11},{9,8},{10,9... | collective-permute-start | bytes 1376264 | tf_op jit(solution)/shard_map/ppermute | solution.py:267
  61.6 19.7 %collective-permute-start.3 = (bf16[256,896]{1,0:T(8,128)(2,1)}, bf16[256,896]{1,0:T(8,128)(2,1)}, u32[]{:S(2)}, u32[]{:S(2)}) collective-permute-start(bf16[256,896]{1,0:T(8,128)(2,1)} %collective-permute-done.2.nb), channel_id=1, source_target_pairs={{0,3},{1,0},{2,1},{3,2},{4,7},{5,4},{6,5},{7,6},{8,11},{9,8},{10,9... | collective-permute-start | bytes 1376264 | tf_op jit(solution)/shard_map/ppermute | solution.py:267
  65.1 19.4 %collective-permute-start.1 = (bf16[256,896]{1,0:T(8,128)(2,1)}, bf16[256,896]{1,0:T(8,128)(2,1)}, u32[]{:S(2)}, u32[]{:S(2)}) collective-permute-start(bf16[256,896]{1,0:T(8,128)(2,1)} %collective-permute-done.pa), channel_id=1, source_target_pairs={{0,1},{1,2},{2,3},{3,0},{4,5},{5,6},{6,7},{7,4},{8,9},{9,10},{10,1... | collective-permute-start | bytes 1376264 | tf_op jit(solution)/shard_map/ppermute | solution.py:267
  67.5 1.1 copy-start.2
  74.6 1.2 copy-start.1
  75.8 1.4 copy-start.3
  87.7 5.4 %copy-start.4 = (bf16[512,768]{1,0:T(8,128)(2,1)}, bf16[512,768]{1,0:T(8,128)(2,1)S(1)}, u32[]{:S(2)}) copy-start(bf16[512,768]{1,0:T(8,128)(2,1)S(1)} %get-tuple-element.44.grads_ref.grads) | copy-start | bytes 2359300
  87.7 5.4 %copy-start.5 = (bf16[512,384]{1,0:T(8,128)(2,1)}, bf16[512,384]{1,0:T(8,128)(2,1)S(1)}, u32[]{:S(2)}) copy-start(bf16[512,384]{1,0:T(8,128)(2,1)S(1)} %get-tuple-element.55.hid) | copy-start | bytes 1179652
  87.7 8.1 %collective-permute-start.11 = (bf16[256,512]{1,0:T(8,128)(2,1)S(1)}, bf16[256,512]{1,0:T(8,128)(2,1)S(1)}, u32[]{:S(2)}, u32[]{:S(2)}) collective-permute-start(bf16[256,512]{1,0:T(8,128)(2,1)S(1)} %get-tuple-element.49), channel_id=1, source_target_pairs={{0,1},{1,2},{2,3},{3,0},{4,5},{5,6},{6,7},{7,4},{8,9},{9,10},{10,1... | collective-permute-start | bytes 786440 | tf_op jit(solution)/shard_map/ppermute | solution.py:267
  88.0 7.8 %collective-permute-start.12 = (bf16[256,512]{1,0:T(8,128)(2,1)S(1)}, bf16[256,512]{1,0:T(8,128)(2,1)S(1)}, u32[]{:S(2)}, u32[]{:S(2)}) collective-permute-start(bf16[256,512]{1,0:T(8,128)(2,1)S(1)} %get-tuple-element.51), channel_id=1, source_target_pairs={{0,3},{1,0},{2,1},{3,2},{4,7},{5,4},{6,5},{7,6},{8,11},{9,8},{10,9... | collective-permute-start | bytes 786440 | tf_op jit(solution)/shard_map/ppermute | solution.py:267
  93.2 45.4 %collective-permute-start.9 = (bf16[256,512]{1,0:T(8,128)(2,1)}, bf16[256,512]{1,0:T(8,128)(2,1)S(1)}, u32[]{:S(2)}, u32[]{:S(2)}) collective-permute-start(bf16[256,512]{1,0:T(8,128)(2,1)} %get-tuple-element.46), channel_id=1, source_target_pairs={{0,1},{1,2},{2,3},{3,0},{4,5},{5,6},{6,7},{7,4},{8,9},{9,10},{10,1... | collective-permute-start | bytes 786440 | tf_op jit(solution)/shard_map/ppermute | solution.py:267
  93.2 45.4 %collective-permute-start.10 = (bf16[256,512]{1,0:T(8,128)(2,1)S(1)}, bf16[256,512]{1,0:T(8,128)(2,1)S(1)}, u32[]{:S(2)}, u32[]{:S(2)}) collective-permute-start(bf16[256,512]{1,0:T(8,128)(2,1)S(1)} %get-tuple-element.47), channel_id=1, source_target_pairs={{0,3},{1,0},{2,1},{3,2},{4,7},{5,4},{6,5},{7,6},{8,11},{9,8},{10,9... | collective-permute-start | bytes 786440 | tf_op jit(solution)/shard_map/ppermute | solution.py:267
  97.1 41.4 %collective-permute-start.13 = (bf16[256,512]{1,0:T(8,128)(2,1)S(1)}, bf16[256,512]{1,0:T(8,128)(2,1)S(1)}, u32[]{:S(2)}, u32[]{:S(2)}) collective-permute-start(bf16[256,512]{1,0:T(8,128)(2,1)S(1)} %get-tuple-element.52), channel_id=1, source_target_pairs={{0,1},{1,2},{2,3},{3,0},{4,5},{5,6},{6,7},{7,4},{8,9},{9,10},{10,1... | collective-permute-start | bytes 786440 | tf_op jit(solution)/shard_map/ppermute | solution.py:267
  97.2 41.3 %collective-permute-start.14 = (bf16[256,512]{1,0:T(8,128)(2,1)S(1)}, bf16[256,512]{1,0:T(8,128)(2,1)S(1)}, u32[]{:S(2)}, u32[]{:S(2)}) collective-permute-start(bf16[256,512]{1,0:T(8,128)(2,1)S(1)} %get-tuple-element.53), channel_id=1, source_target_pairs={{0,3},{1,0},{2,1},{3,2},{4,7},{5,4},{6,5},{7,6},{8,11},{9,8},{10,9... | collective-permute-start | bytes 786440 | tf_op jit(solution)/shard_map/ppermute | solution.py:267
  99.9 5.0 %collective-permute-start.8 = (f32[64,128]{1,0:T(8,128)S(1)}, f32[64,128]{1,0:T(8,128)S(1)}, u32[]{:S(2)}, u32[]{:S(2)}) collective-permute-start(f32[64,128]{1,0:T(8,128)S(1)} %get-tuple-element.40.a), channel_id=1, source_target_pairs={{0,2},{1,3},{2,0},{3,1},{4,6},{5,7},{6,4},{7,5},{8,10},{9,11},{10,... | collective-permute-start | bytes 98312 | tf_op jit(solution)/shard_map/ppermute | solution.py:267
  104.9 4.6 %collective-permute-start.7 = (f32[64,128]{1,0:T(8,128)S(1)}, f32[64,128]{1,0:T(8,128)S(1)}, u32[]{:S(2)}, u32[]{:S(2)}) collective-permute-start(f32[64,128]{1,0:T(8,128)S(1)} %get-tuple-element.40.a), channel_id=1, source_target_pairs={{0,3},{1,0},{2,1},{3,2},{4,7},{5,4},{6,5},{7,6},{8,11},{9,8},{10,9... | collective-permute-start | bytes 98312 | tf_op jit(solution)/shard_map/ppermute | solution.py:267
  109.5 4.3 %collective-permute-start.6 = (f32[64,128]{1,0:T(8,128)S(1)}, f32[64,128]{1,0:T(8,128)S(1)}, u32[]{:S(2)}, u32[]{:S(2)}) collective-permute-start(f32[64,128]{1,0:T(8,128)S(1)} %get-tuple-element.40.a), channel_id=1, source_target_pairs={{0,1},{1,2},{2,3},{3,0},{4,5},{5,6},{6,7},{7,4},{8,9},{9,10},{10,1... | collective-permute-start | bytes 98312 | tf_op jit(solution)/shard_map/ppermute | solution.py:267
  114.3 24.2 %all-to-all-start.2 = ((f32[64,1,128]{2,1,0:T(1,128)}), f32[64,1,128]{2,1,0:T(1,128)S(1)}, u32[]{:S(2)}, u32[]{:S(2)}) async-start(f32[64,1,128]{2,1,0:T(1,128)} %bitcast.13), calls=%async_computation.2 | async-start | bytes 65536 | tf_op jit(solution)/shard_map/all_to_all | solution.py:270
  142.3 25.2 %all-to-all-start.3 = ((bf16[64,8,640]{2,1,0:T(8,128)(2,1)}), bf16[64,8,640]{2,1,0:T(8,128)(2,1)S(1)}, u32[]{:S(2)}, u32[]{:S(2)}) async-start(bf16[64,8,640]{2,1,0:T(8,128)(2,1)} %get-tuple-element.54), calls=%async_computation.3 | async-start | bytes 1310720 | tf_op jit(solution)/shard_map/all_to_all | solution.py:270
  (1 other events, 0.6 us)

commit v2 on v1

--- a/solution.py
+++ b/solution.py
@@ -306,7 +306,7 @@
     )(*(pltpu.with_memory_space_constraint(w[0], pltpu.HBM) for w in (w_gate, w_up, w_down)))
 
     near = call(
-        functools.partial(near_kernel, share), [shape((rows, 2 * ff), F32), shape((rows, ff), F32)], 9 * unit
+        functools.partial(near_kernel, share), [shape((rows, 2 * ff), F32), shape((rows, ff), F32)], 9 * unit, raw=(0,)
     )(me, own, pa, pb, na, nb, more, wgu, wd)
     hid, grads, score, b2a, b2b = call(
         functools.partial(far_kernel, cap),
@@ -319,10 +319,9 @@
         token_kernel,
         [shape((half, share), F32)] * 2 + [shape((rows, share), F32)] + [shape((half, share), BF16)] * 2,
         6 * unit,
-        to_hbm=3,
     )(me, grads, wgu)
     d1, d2 = hop(b1b, 1), hop(b3a, -1)
-    ahead, behind = call(onward_kernel, [shape((half, share), BF16)] * 2, 1, scalar=False, raw=(0, 2))(b1a, s1, b3b, s2)
+    ahead, behind = call(onward_kernel, [shape((half, share), BF16)] * 2, 1, scalar=False)(b1a, s1, b3b, s2)
     e1, e2 = hop(ahead, 1), hop(behind, -1)
     (gate,) = call(mark_kernel, [shape((n_tok, experts), F32)], 1, scalar=False)(gate)
     (score,) = call(total_kernel, [shape((peers, 128), F32)], 1, scalar=False)(
@@ -334,7 +333,6 @@
         [shape((peers, cap, share + 128), BF16), shape((n_tok, experts), F32)],
         unit,
         scalar=False,
-        raw=(4,),
     )(q, code, gate, mine, b0, d1, d2, e1, e2)
     home = exchange(payload)
     gwg, gwu, gwd, part = call(

time: 169 us -> 167 us (0.988)
  Pallas kernels: 28.7 us -> 25.5 us
  waiting for transfers between devices: 47.7 us -> 50.3 us
    pallas_call x10, Pallas kernels: 26.3 us -> 23.1 us  [run(): pl.pallas_call(body, out_shape=[(pltpu.HBM if i < to_hbm else pltpu.VMEM)...]
    ppermute x15, waiting for transfers between devices: 25.4 us -> 28 us  [hop(): return lax.ppermute(value, 'tp', [(i, (i + by) % tp) for i in range(tp)])]
    unnamed x14 -> x16, local copies, waits for them, and re-layouts: 4.34 us -> 3.53 us
  transfers between devices with their start and end apart: 18 -> 18, of which waited for: 9 -> 9; matrix products, arithmetic and copies ran while one was open for 1% -> 1% of each run, Pallas kernels for 11% -> 10%
where the time goes in v2:
time: 167 us
  waiting for transfers between devices  50.3 us (30%)
  starting transfers between devices  47.1 us (28%)
  blocking collectives  38.5 us (23%)
  Pallas kernels  25.5 us (15%)
  local copies, waits for them, and re-layouts  4.54 us (3%)
    all_to_all x1, blocking collectives, exchange(): return lax.all_to_all(value, 'ep', split_axis=0, concat_axis=0, tiled=True)  38.5 us
    ppermute x15, waiting for transfers between devices, hop(): return lax.ppermute(value, 'tp', [(i, (i + by) % tp) for i in range(tp)])  28 us
    all_to_all x3, starting transfers between devices, exchange(): return lax.all_to_all(value, 'ep', split_axis=0, concat_axis=0, tiled=True)  26 us
    pallas_call x10, Pallas kernels, run(): pl.pallas_call(body, out_shape=[(pltpu.HBM if i < to_hbm else pltpu.VMEM)...  23.1 us
    all_to_all x3, waiting for transfers between devices, exchange(): return lax.all_to_all(value, 'ep', split_axis=0, concat_axis=0, tiled=True)  22.3 us
    ppermute x15, starting transfers between devices, hop(): return lax.ppermute(value, 'tp', [(i, (i + by) % tp) for i in range(tp)])  21.1 us
    unnamed x16, local copies, waits for them, and re-layouts  3.53 us
  transfers between devices with their start and end apart: 18, of which 9 were waited for; matrix products, arithmetic and copies ran while one was open for 1% of the time, Pallas kernels for 10%

profile of v2, /device:TPU:1, one launch (start us, length us, event | category | flops | bytes accessed | tf_op | source)
XLA Modules:
  0.0 166.7 jit_solution(14416353935287000674)
XLA Ops:
  0.6 3.1 %shard_map.110 = (bf16[512,896]{1,0:T(8,128)(2,1)S(1)}, bf16[512,512]{1,0:T(8,128)(2,1)}, f32[48,64]{1,0:T(8,128)S(1)}, f32[48,64]{1,0:T(8,128)S(1)}, bf16[48,512]{1,0:T(8,128)(2,1)S(1)}) custom-call(s32[1]{0:T(128)} %bitcast.tp_ref, bf16[48,2048]{1,0:T(8,128)(2,1)} %tok_ref.1, bf16[48,2048]{1,0:T(8,128)(2,1)} %og_ref.1, s32[4,48]{1,0:T(4,128)} %bitcast.31, ...), custom_call_target="tpu_custom_call" | custom-call | flops 201326592 | bytes 4194304 | tf_op jit(solution)/shard_map/pallas_call | solution.py:236
  3.7 38.5 %all_to_all.20 = bf16[64,8,896]{2,1,0:T(8,128)(2,1)S(1)} all-to-all(bf16[64,8,896]{2,1,0:T(8,128)(2,1)S(1)} %bitcast.22), channel_id=1, replica_groups=mesh['ep'=64,'tp'=4] {'ep'}, dimensions={0} | all-to-all | bytes 1835008 | tf_op jit(solution)/shard_map/all_to_all | solution.py:270
  42.2 6.3 %all-to-all-start.1 = ((bf16[64,8,512]{2,1,0:T(8,128)(2,1)}), bf16[64,8,512]{2,1,0:T(8,128)(2,1)}, u32[]{:S(2)}, u32[]{:S(2)}) async-start(bf16[64,8,512]{2,1,0:T(8,128)(2,1)} %bitcast.7), calls=%async_computation.1 | async-start | bytes 1048576 | tf_op jit(solution)/shard_map/all_to_all | solution.py:270
  49.5 2.5 %collective-permute-start.2 = (bf16[256,896]{1,0:T(8,128)(2,1)}, bf16[256,896]{1,0:T(8,128)(2,1)}, u32[]{:S(2)}, u32[]{:S(2)}) collective-permute-start(bf16[256,896]{1,0:T(8,128)(2,1)} %get-tuple-element.63), channel_id=1, source_target_pairs={{0,3},{1,0},{2,1},{3,2},{4,7},{5,4},{6,5},{7,6},{8,11},{9,8},{10,9... | collective-permute-start | bytes 1376264 | tf_op jit(solution)/shard_map/ppermute | solution.py:267
  52.2 2.5 %collective-permute-start.5 = (bf16[256,896]{1,0:T(8,128)(2,1)}, bf16[256,896]{1,0:T(8,128)(2,1)}, u32[]{:S(2)}, u32[]{:S(2)}) collective-permute-start(bf16[256,896]{1,0:T(8,128)(2,1)} %get-tuple-element.64), channel_id=1, source_target_pairs={{0,3},{1,0},{2,1},{3,2},{4,7},{5,4},{6,5},{7,6},{8,11},{9,8},{10,9... | collective-permute-start | bytes 1376264 | tf_op jit(solution)/shard_map/ppermute | solution.py:267
  54.7 7.0 %collective-permute-done.2.nb = bf16[256,896]{1,0:T(8,128)(2,1)} collective-permute-done((bf16[256,896]{1,0:T(8,128)(2,1)}, bf16[256,896]{1,0:T(8,128)(2,1)}, u32[]{:S(2)}, u32[]{:S(2)}) %collective-permute-start.2) | collective-permute-done | bytes 458784 | tf_op jit(solution)/shard_map/ppermute | solution.py:267
  61.7 3.4 %collective-permute-start.3 = (bf16[256,896]{1,0:T(8,128)(2,1)}, bf16[256,896]{1,0:T(8,128)(2,1)}, u32[]{:S(2)}, u32[]{:S(2)}) collective-permute-start(bf16[256,896]{1,0:T(8,128)(2,1)} %collective-permute-done.2.nb), channel_id=1, source_target_pairs={{0,3},{1,0},{2,1},{3,2},{4,7},{5,4},{6,5},{7,6},{8,11},{9,8},{10,9... | collective-permute-start | bytes 1376264 | tf_op jit(solution)/shard_map/ppermute | solution.py:267
  65.1 2.4 %shard_map.111 = (bf16[2048,768]{1,0:T(8,128)(2,1)S(1)}, bf16[384,2048]{1,0:T(8,128)(2,1)S(1)}) custom-call(bf16[2048,384]{1,0:T(8,128)(2,1)} %bitcast.26, bf16[2048,384]{1,0:T(8,128)(2,1)} %bitcast.27, bf16[384,2048]{1,0:T(8,128)(2,1)} %bitcast.28), custom_call_target="tpu_custom_call" | custom-call | flops 201326592 | bytes 4194304 | tf_op jit(solution)/shard_map/pallas_call | solution.py:298
  68.6 6.0 %collective-permute-done.4.pb = bf16[256,896]{1,0:T(8,128)(2,1)} collective-permute-done((bf16[256,896]{1,0:T(8,128)(2,1)}, bf16[256,896]{1,0:T(8,128)(2,1)}, u32[]{:S(2)}, u32[]{:S(2)}) %collective-permute-start.4) | collective-permute-done | bytes 458784 | tf_op jit(solution)/shard_map/ppermute | solution.py:267
  76.0 4.3 %shard_map.112 = (f32[512,768]{1,0:T(8,128)S(1)}, f32[512,384]{1,0:T(8,128)S(1)}) custom-call(s32[1]{0:T(128)} %bitcast.tp_ref, bf16[512,896]{1,0:T(8,128)(2,1)} %bitcast.24, bf16[256,896]{1,0:T(8,128)(2,1)} %collective-permute-done.pa, bf16[256,896]{1,0:T(8,128)(2,1)} %collective-permute-done.4.pb, bf16[256,896]{1,0:T(8,128)(2,1)} %collective-permute-done.5.na, ...), custom_call_target="tpu_custom_call" | custom-call | flops 1811939328 | bytes 4194304 | tf_op jit(solution)/shard_map/pallas_call | solution.py:236
  81.3 3.1 %collective-permute-done.1.f0 = bf16[256,896]{1,0:T(8,128)(2,1)} collective-permute-done((bf16[256,896]{1,0:T(8,128)(2,1)}, bf16[256,896]{1,0:T(8,128)(2,1)}, u32[]{:S(2)}, u32[]{:S(2)}) %collective-permute-start.1) | collective-permute-done | bytes 458784 | tf_op jit(solution)/shard_map/ppermute | solution.py:267
  84.5 3.3 %shard_map.113 = (bf16[512,384]{1,0:T(8,128)(2,1)S(1)}, bf16[512,768]{1,0:T(8,128)(2,1)S(1)}, f32[64,128]{1,0:T(8,128)S(1)}, bf16[256,512]{1,0:T(8,128)(2,1)S(1)}, bf16[256,512]{1,0:T(8,128)(2,1)S(1)}) custom-call(s32[1]{0:T(128)} %bitcast.tp_ref, bf16[256,896]{1,0:T(8,128)(2,1)} %collective-permute-done.1.f0, bf16[256,896]{1,0:T(8,128)(2,1)} %collective-permute-done.3.f1, ...), custom_call_target="tpu_custom_call" | custom-call | flops 1006632960 | bytes 4194304 | tf_op jit(solution)/shard_map/pallas_call | solution.py:236
  88.0 2.7 %collective-permute-start.12 = (bf16[256,512]{1,0:T(8,128)(2,1)S(1)}, bf16[256,512]{1,0:T(8,128)(2,1)S(1)}, u32[]{:S(2)}, u32[]{:S(2)}) collective-permute-start(bf16[256,512]{1,0:T(8,128)(2,1)S(1)} %get-tuple-element.51), channel_id=1, source_target_pairs={{0,3},{1,0},{2,1},{3,2},{4,7},{5,4},{6,5},{7,6},{8,11},{9,8},{10,9... | collective-permute-start | bytes 786440 | tf_op jit(solution)/shard_map/ppermute | solution.py:267
  93.1 2.7 %collective-permute-start.10 = (bf16[256,512]{1,0:T(8,128)(2,1)S(1)}, bf16[256,512]{1,0:T(8,128)(2,1)S(1)}, u32[]{:S(2)}, u32[]{:S(2)}) collective-permute-start(bf16[256,512]{1,0:T(8,128)(2,1)S(1)} %get-tuple-element.47), channel_id=1, source_target_pairs={{0,3},{1,0},{2,1},{3,2},{4,7},{5,4},{6,5},{7,6},{8,11},{9,8},{10,9... | collective-permute-start | bytes 786440 | tf_op jit(solution)/shard_map/ppermute | solution.py:267
  96.0 2.7 %collective-permute-start.14 = (bf16[256,512]{1,0:T(8,128)(2,1)S(1)}, bf16[256,512]{1,0:T(8,128)(2,1)S(1)}, u32[]{:S(2)}, u32[]{:S(2)}) collective-permute-start(bf16[256,512]{1,0:T(8,128)(2,1)S(1)} %get-tuple-element.53), channel_id=1, source_target_pairs={{0,3},{1,0},{2,1},{3,2},{4,7},{5,4},{6,5},{7,6},{8,11},{9,8},{10,9... | collective-permute-start | bytes 786440 | tf_op jit(solution)/shard_map/ppermute | solution.py:267
  99.2 6.6 %collective-permute-done.8.d = f32[64,128]{1,0:T(8,128)S(1)} collective-permute-done((f32[64,128]{1,0:T(8,128)S(1)}, f32[64,128]{1,0:T(8,128)S(1)}, u32[]{:S(2)}, u32[]{:S(2)}) %collective-permute-start.8) | collective-permute-done | bytes 32800 | tf_op jit(solution)/shard_map/ppermute | solution.py:267
  105.7 2.7 %collective-permute-start.7 = (f32[64,128]{1,0:T(8,128)S(1)}, f32[64,128]{1,0:T(8,128)S(1)}, u32[]{:S(2)}, u32[]{:S(2)}) collective-permute-start(f32[64,128]{1,0:T(8,128)S(1)} %get-tuple-element.40.a), channel_id=1, source_target_pairs={{0,3},{1,0},{2,1},{3,2},{4,7},{5,4},{6,5},{7,6},{8,11},{9,8},{10,9... | collective-permute-start | bytes 98312 | tf_op jit(solution)/shard_map/ppermute | solution.py:267
  110.4 3.3 %collective-permute-done.6.b = f32[64,128]{1,0:T(8,128)S(1)} collective-permute-done((f32[64,128]{1,0:T(8,128)S(1)}, f32[64,128]{1,0:T(8,128)S(1)}, u32[]{:S(2)}, u32[]{:S(2)}) %collective-permute-start.6) | collective-permute-done | bytes 32800 | tf_op jit(solution)/shard_map/ppermute | solution.py:267
  114.3 14.9 %all-to-all-start.2 = ((f32[64,1,128]{2,1,0:T(1,128)}), f32[64,1,128]{2,1,0:T(1,128)S(1)}, u32[]{:S(2)}, u32[]{:S(2)}) async-start(f32[64,1,128]{2,1,0:T(1,128)} %bitcast.13), calls=%async_computation.2 | async-start | bytes 65536 | tf_op jit(solution)/shard_map/all_to_all | solution.py:270
  129.2 9.3 %all-to-all-done.2 = f32[64,1,128]{2,1,0:T(1,128)S(1)} async-done(((f32[64,1,128]{2,1,0:T(1,128)}), f32[64,1,128]{2,1,0:T(1,128)S(1)}, u32[]{:S(2)}, u32[]{:S(2)}) %all-to-all-start.2) | async-done | bytes 32800 | tf_op jit(solution)/shard_map/all_to_all | solution.py:270
  138.6 1.9 %shard_map.118 = (bf16[64,8,640]{2,1,0:T(8,128)(2,1)}, f32[48,64]{1,0:T(8,128)S(1)}) custom-call(f32[64,128]{1,0:T(8,128)S(1)} %bitcast.23, f32[48,64]{1,0:T(8,128)S(1)} %get-tuple-element.41.code_ref, f32[48,64]{1,0:T(8,128)S(1)} %shard_map.115.gate_ref, bf16[48,512]{1,0:T(8,128)(2,1)S(1)} %get-tuple-element.43.tok_ref, f32[512,512]{1,0:T(8,128)S(1)} %copy-done.3, ...), custom_call_target="tpu_custom_call" | custom-call | flops 201326592 | bytes 4194304 | tf_op jit(solution)/shard_map/pallas_call | solution.py:236
  140.5 4.8 %all-to-all-start.3 = ((bf16[64,8,640]{2,1,0:T(8,128)(2,1)}), bf16[64,8,640]{2,1,0:T(8,128)(2,1)S(1)}, u32[]{:S(2)}, u32[]{:S(2)}) async-start(bf16[64,8,640]{2,1,0:T(8,128)(2,1)} %get-tuple-element.54), calls=%async_computation.3 | async-start | bytes 1310720 | tf_op jit(solution)/shard_map/all_to_all | solution.py:270
  145.3 7.5 %shard_map.119 = (bf16[2048,384]{1,0:T(8,128)(2,1)}, bf16[2048,384]{1,0:T(8,128)(2,1)}, bf16[384,2048]{1,0:T(8,128)(2,1)}, f32[48,512]{1,0:T(8,128)S(1)}) custom-call(s32[1]{0:T(128)} %bitcast.tp_ref, bf16[512,896]{1,0:T(8,128)(2,1)} %bitcast.25, bf16[256,896]{1,0:T(8,128)(2,1)} %collective-permute-done.pa, bf16[256,896]{1,0:T(8,128)(2,1)} %collective-permute-done.4.pb, ...), custom_call_target="tpu_custom_call" | custom-call | flops 2415919104 | bytes 4194304 | tf_op jit(solution)/shard_map/pallas_call | solution.py:236
  152.8 13.0 %all-to-all-done.3.home_ref = bf16[64,8,640]{2,1,0:T(8,128)(2,1)S(1)} async-done(((bf16[64,8,640]{2,1,0:T(8,128)(2,1)}), bf16[64,8,640]{2,1,0:T(8,128)(2,1)S(1)}, u32[]{:S(2)}, u32[]{:S(2)}) %all-to-all-start.3) | async-done | bytes 655392 | tf_op jit(solution)/shard_map/all_to_all | solution.py:270
  (41 shorter events, 11.7 us)
Async XLA Ops:
  42.2 22.9 %copy-start.7 = (bf16[64,8,896]{2,1,0:T(8,128)(2,1)}, bf16[64,8,896]{2,1,0:T(8,128)(2,1)S(1)}, u32[]{:S(2)}) copy-start(bf16[64,8,896]{2,1,0:T(8,128)(2,1)S(1)} %all_to_all.20) | copy-start | bytes 2752516
  42.2 26.4 %all-to-all-start.1 = ((bf16[64,8,512]{2,1,0:T(8,128)(2,1)}), bf16[64,8,512]{2,1,0:T(8,128)(2,1)}, u32[]{:S(2)}, u32[]{:S(2)}) async-start(bf16[64,8,512]{2,1,0:T(8,128)(2,1)} %bitcast.7), calls=%async_computation.1 | async-start | bytes 1048576 | tf_op jit(solution)/shard_map/all_to_all | solution.py:270
  49.5 12.1 %collective-permute-start.2 = (bf16[256,896]{1,0:T(8,128)(2,1)}, bf16[256,896]{1,0:T(8,128)(2,1)}, u32[]{:S(2)}, u32[]{:S(2)}) collective-permute-start(bf16[256,896]{1,0:T(8,128)(2,1)} %get-tuple-element.63), channel_id=1, source_target_pairs={{0,3},{1,0},{2,1},{3,2},{4,7},{5,4},{6,5},{7,6},{8,11},{9,8},{10,9... | collective-permute-start | bytes 1376264 | tf_op jit(solution)/shard_map/ppermute | solution.py:267
  52.0 13.1 %collective-permute-start = (bf16[256,896]{1,0:T(8,128)(2,1)}, bf16[256,896]{1,0:T(8,128)(2,1)}, u32[]{:S(2)}, u32[]{:S(2)}) collective-permute-start(bf16[256,896]{1,0:T(8,128)(2,1)} %get-tuple-element.64), channel_id=1, source_target_pairs={{0,1},{1,2},{2,3},{3,0},{4,5},{5,6},{6,7},{7,4},{8,9},{9,10},{10,1... | collective-permute-start | bytes 1376264 | tf_op jit(solution)/shard_map/ppermute | solution.py:267
  52.0 22.6 %collective-permute-start.4 = (bf16[256,896]{1,0:T(8,128)(2,1)}, bf16[256,896]{1,0:T(8,128)(2,1)}, u32[]{:S(2)}, u32[]{:S(2)}) collective-permute-start(bf16[256,896]{1,0:T(8,128)(2,1)} %get-tuple-element.63), channel_id=1, source_target_pairs={{0,1},{1,2},{2,3},{3,0},{4,5},{5,6},{6,7},{7,4},{8,9},{9,10},{10,1... | collective-permute-start | bytes 1376264 | tf_op jit(solution)/shard_map/ppermute | solution.py:267
  52.2 22.4 %collective-permute-start.5 = (bf16[256,896]{1,0:T(8,128)(2,1)}, bf16[256,896]{1,0:T(8,128)(2,1)}, u32[]{:S(2)}, u32[]{:S(2)}) collective-permute-start(bf16[256,896]{1,0:T(8,128)(2,1)} %get-tuple-element.64), channel_id=1, source_target_pairs={{0,3},{1,0},{2,1},{3,2},{4,7},{5,4},{6,5},{7,6},{8,11},{9,8},{10,9... | collective-permute-start | bytes 1376264 | tf_op jit(solution)/shard_map/ppermute | solution.py:267
  61.7 19.7 %collective-permute-start.3 = (bf16[256,896]{1,0:T(8,128)(2,1)}, bf16[256,896]{1,0:T(8,128)(2,1)}, u32[]{:S(2)}, u32[]{:S(2)}) collective-permute-start(bf16[256,896]{1,0:T(8,128)(2,1)} %collective-permute-done.2.nb), channel_id=1, source_target_pairs={{0,3},{1,0},{2,1},{3,2},{4,7},{5,4},{6,5},{7,6},{8,11},{9,8},{10,9... | collective-permute-start | bytes 1376264 | tf_op jit(solution)/shard_map/ppermute | solution.py:267
  65.1 19.4 %collective-permute-start.1 = (bf16[256,896]{1,0:T(8,128)(2,1)}, bf16[256,896]{1,0:T(8,128)(2,1)}, u32[]{:S(2)}, u32[]{:S(2)}) collective-permute-start(bf16[256,896]{1,0:T(8,128)(2,1)} %collective-permute-done.pa), channel_id=1, source_target_pairs={{0,1},{1,2},{2,3},{3,0},{4,5},{5,6},{6,7},{7,4},{8,9},{9,10},{10,1... | collective-permute-start | bytes 1376264 | tf_op jit(solution)/shard_map/ppermute | solution.py:267
  74.6 1.4 copy-start.1
  87.7 4.4 %copy-start.4 = (bf16[512,768]{1,0:T(8,128)(2,1)}, bf16[512,768]{1,0:T(8,128)(2,1)S(1)}, u32[]{:S(2)}) copy-start(bf16[512,768]{1,0:T(8,128)(2,1)S(1)} %get-tuple-element.44.grads_ref.grads) | copy-start | bytes 2359300
  87.7 4.4 %copy-start.5 = (bf16[512,384]{1,0:T(8,128)(2,1)}, bf16[512,384]{1,0:T(8,128)(2,1)S(1)}, u32[]{:S(2)}) copy-start(bf16[512,384]{1,0:T(8,128)(2,1)S(1)} %get-tuple-element.55.hid) | copy-start | bytes 1179652
  87.7 8.0 %collective-permute-start.11 = (bf16[256,512]{1,0:T(8,128)(2,1)S(1)}, bf16[256,512]{1,0:T(8,128)(2,1)S(1)}, u32[]{:S(2)}, u32[]{:S(2)}) collective-permute-start(bf16[256,512]{1,0:T(8,128)(2,1)S(1)} %get-tuple-element.49), channel_id=1, source_target_pairs={{0,1},{1,2},{2,3},{3,0},{4,5},{5,6},{6,7},{7,4},{8,9},{9,10},{10,1... | collective-permute-start | bytes 786440 | tf_op jit(solution)/shard_map/ppermute | solution.py:267
  88.0 7.8 %collective-permute-start.12 = (bf16[256,512]{1,0:T(8,128)(2,1)S(1)}, bf16[256,512]{1,0:T(8,128)(2,1)S(1)}, u32[]{:S(2)}, u32[]{:S(2)}) collective-permute-start(bf16[256,512]{1,0:T(8,128)(2,1)S(1)} %get-tuple-element.51), channel_id=1, source_target_pairs={{0,3},{1,0},{2,1},{3,2},{4,7},{5,4},{6,5},{7,6},{8,11},{9,8},{10,9... | collective-permute-start | bytes 786440 | tf_op jit(solution)/shard_map/ppermute | solution.py:267
  93.1 45.5 %copy-start.3 = (f32[512,512]{1,0:T(8,128)S(1)}, f32[512,512]{1,0:T(8,128)}, u32[]{:S(2)}) copy-start(f32[512,512]{1,0:T(8,128)} %copy-done.2) | copy-start | bytes 3145732
  93.1 45.5 %collective-permute-start.9 = (bf16[256,512]{1,0:T(8,128)(2,1)}, bf16[256,512]{1,0:T(8,128)(2,1)S(1)}, u32[]{:S(2)}, u32[]{:S(2)}) collective-permute-start(bf16[256,512]{1,0:T(8,128)(2,1)} %get-tuple-element.46), channel_id=1, source_target_pairs={{0,1},{1,2},{2,3},{3,0},{4,5},{5,6},{6,7},{7,4},{8,9},{9,10},{10,1... | collective-permute-start | bytes 786440 | tf_op jit(solution)/shard_map/ppermute | solution.py:267
  93.1 45.5 %collective-permute-start.10 = (bf16[256,512]{1,0:T(8,128)(2,1)S(1)}, bf16[256,512]{1,0:T(8,128)(2,1)S(1)}, u32[]{:S(2)}, u32[]{:S(2)}) collective-permute-start(bf16[256,512]{1,0:T(8,128)(2,1)S(1)} %get-tuple-element.47), channel_id=1, source_target_pairs={{0,3},{1,0},{2,1},{3,2},{4,7},{5,4},{6,5},{7,6},{8,11},{9,8},{10,9... | collective-permute-start | bytes 786440 | tf_op jit(solution)/shard_map/ppermute | solution.py:267
  95.9 42.7 %collective-permute-start.13 = (bf16[256,512]{1,0:T(8,128)(2,1)S(1)}, bf16[256,512]{1,0:T(8,128)(2,1)S(1)}, u32[]{:S(2)}, u32[]{:S(2)}) collective-permute-start(bf16[256,512]{1,0:T(8,128)(2,1)S(1)} %get-tuple-element.52), channel_id=1, source_target_pairs={{0,1},{1,2},{2,3},{3,0},{4,5},{5,6},{6,7},{7,4},{8,9},{9,10},{10,1... | collective-permute-start | bytes 786440 | tf_op jit(solution)/shard_map/ppermute | solution.py:267
  96.0 42.6 %collective-permute-start.14 = (bf16[256,512]{1,0:T(8,128)(2,1)S(1)}, bf16[256,512]{1,0:T(8,128)(2,1)S(1)}, u32[]{:S(2)}, u32[]{:S(2)}) collective-permute-start(bf16[256,512]{1,0:T(8,128)(2,1)S(1)} %get-tuple-element.53), channel_id=1, source_target_pairs={{0,3},{1,0},{2,1},{3,2},{4,7},{5,4},{6,5},{7,6},{8,11},{9,8},{10,9... | collective-permute-start | bytes 786440 | tf_op jit(solution)/shard_map/ppermute | solution.py:267
  98.6 7.1 %collective-permute-start.8 = (f32[64,128]{1,0:T(8,128)S(1)}, f32[64,128]{1,0:T(8,128)S(1)}, u32[]{:S(2)}, u32[]{:S(2)}) collective-permute-start(f32[64,128]{1,0:T(8,128)S(1)} %get-tuple-element.40.a), channel_id=1, source_target_pairs={{0,2},{1,3},{2,0},{3,1},{4,6},{5,7},{6,4},{7,5},{8,10},{9,11},{10,... | collective-permute-start | bytes 98312 | tf_op jit(solution)/shard_map/ppermute | solution.py:267
  105.7 3.7 %collective-permute-start.7 = (f32[64,128]{1,0:T(8,128)S(1)}, f32[64,128]{1,0:T(8,128)S(1)}, u32[]{:S(2)}, u32[]{:S(2)}) collective-permute-start(f32[64,128]{1,0:T(8,128)S(1)} %get-tuple-element.40.a), channel_id=1, source_target_pairs={{0,3},{1,0},{2,1},{3,2},{4,7},{5,4},{6,5},{7,6},{8,11},{9,8},{10,9... | collective-permute-start | bytes 98312 | tf_op jit(solution)/shard_map/ppermute | solution.py:267
  109.4 4.3 %collective-permute-start.6 = (f32[64,128]{1,0:T(8,128)S(1)}, f32[64,128]{1,0:T(8,128)S(1)}, u32[]{:S(2)}, u32[]{:S(2)}) collective-permute-start(f32[64,128]{1,0:T(8,128)S(1)} %get-tuple-element.40.a), channel_id=1, source_target_pairs={{0,1},{1,2},{2,3},{3,0},{4,5},{5,6},{6,7},{7,4},{8,9},{9,10},{10,1... | collective-permute-start | bytes 98312 | tf_op jit(solution)/shard_map/ppermute | solution.py:267
  114.3 24.3 %all-to-all-start.2 = ((f32[64,1,128]{2,1,0:T(1,128)}), f32[64,1,128]{2,1,0:T(1,128)S(1)}, u32[]{:S(2)}, u32[]{:S(2)}) async-start(f32[64,1,128]{2,1,0:T(1,128)} %bitcast.13), calls=%async_computation.2 | async-start | bytes 65536 | tf_op jit(solution)/shard_map/all_to_all | solution.py:270
  140.5 4.8 %copy-start.6 = (f32[48,64]{1,0:T(8,128)}, f32[48,64]{1,0:T(8,128)S(1)}, u32[]{:S(2)}) copy-start(f32[48,64]{1,0:T(8,128)S(1)} %get-tuple-element.56.d_logits_ref) | copy-start | bytes 36868
  140.5 25.2 %all-to-all-start.3 = ((bf16[64,8,640]{2,1,0:T(8,128)(2,1)}), bf16[64,8,640]{2,1,0:T(8,128)(2,1)S(1)}, u32[]{:S(2)}, u32[]{:S(2)}) async-start(bf16[64,8,640]{2,1,0:T(8,128)(2,1)} %get-tuple-element.54), calls=%async_computation.3 | async-start | bytes 1310720 | tf_op jit(solution)/shard_map/all_to_all | solution.py:270
  (2 other events, 2.1 us)

commit v3 on v2

--- a/solution.py
+++ b/solution.py
@@ -37,7 +37,23 @@
     return ((iota((rows, experts), 0) >> bits(cap)) == iota((rows, experts), 1)).astype(F32)
 
 
-def dispatch_kernel(cap, tp_ref, tok_ref, og_ref, ids_ref, rw_ref, send_ref, more_ref, code_ref, gate_ref, mine_ref):
+def slots(cap, code, gate):
+    n_tok, experts = code.shape
+    rows = experts * cap
+    expand = spread(experts, cap).astype(BF16)
+    code_of = mm(expand, code.astype(BF16), NT)
+    pick = code_of == ((iota((rows, n_tok), 0) & (cap - 1)) + 1).astype(F32)
+    gate_of, rest = None, gate
+    for _ in range(3):
+        piece = rest.astype(BF16)
+        rest = rest - piece.astype(F32)
+        term = mm(expand, piece, NT)
+        gate_of = term if gate_of is None else gate_of + term
+    gate_of = jnp.sum(jnp.where(pick, gate_of, 0.0), axis=1, keepdims=True)
+    return pick.astype(F32).astype(BF16), gate_of
+
+
+def dispatch_kernel(cap, tp_ref, tok_ref, og_ref, ids_ref, rw_ref, send_ref, code_ref, gate_ref, mine_ref):
     n_tok = tok_ref.shape[0]
     experts = rw_ref.shape[0]
     share = mine_ref.shape[1]
@@ -57,26 +73,21 @@
     code = mask * (rank + 1.0)
     code_ref[...] = code
     gate_ref[...] = gate
-    expand = spread(experts, cap).astype(BF16)
-    rows = experts * cap
-    code_of = mm(expand, code.astype(BF16), NT)
-    pick = code_of == ((iota((rows, n_tok), 0) & (cap - 1)) + 1).astype(F32)
-    gate_of, rest = None, gate
-    for _ in range(3):
-        piece = rest.astype(BF16)
-        rest = rest - piece.astype(F32)
-        term = mm(expand, piece, NT)
-        gate_of = term if gate_of is None else gate_of + term
-    gate_of = jnp.sum(jnp.where(pick, gate_of, 0.0), axis=1, keepdims=True)
+    pick, gate_of = slots(cap, code, gate)
     mine = tok_ref[:, pl.ds(start, share)]
     mine_ref[...] = mine
     relay = send_ref.shape[1] - share
-    cots = [og_ref[:, pl.ds(start, relay)]]
-    cots += [og_ref[:, j + relay : j + share] for j in range(0, og_ref.shape[1], share)]
-    both = mm(pick.astype(F32).astype(BF16), jnp.concatenate([mine] + cots, axis=1), NN)
+    both = mm(pick, jnp.concatenate([mine, og_ref[:, pl.ds(start, relay)]], axis=1), NN)
     send_ref[:, :share] = both[:, :share].astype(BF16)
-    send_ref[:, share:] = (both[:, share : share + relay] * gate_of).astype(BF16)
-    more_ref[...] = (both[:, share + relay :] * gate_of).astype(BF16)
+    send_ref[:, share:] = (both[:, share:] * gate_of).astype(BF16)
+
+
+def direct_kernel(cap, share, code_ref, gate_ref, og_ref, more_ref):
+    width = og_ref.shape[1]
+    part = more_ref.shape[1] * share // width
+    pick, gate_of = slots(cap, code_ref[...], gate_ref[...])
+    cots = [og_ref[:, j - part : j] for j in range(share, width + 1, share)]
+    more_ref[...] = (mm(pick, jnp.concatenate(cots, axis=1), NN) * gate_of).astype(BF16)
 
 
 def joined(refs, cols):
@@ -119,17 +130,16 @@
     return hidden.astype(BF16), grads, mm(group, spot, NN, HI)
 
 
-def near_kernel(share, tp_ref, own, pa, pb, na, nb, more, wgu, wd, pre, bk):
+def near_kernel(share, tp_ref, own, pa, pb, na, nb, wgu, wd, pre, bk):
     groups = ((0, (own,)), (3, (pa, pb)), (1, (na, nb)))
-    relay = own.shape[1] - share
+    pre[...], bk[...] = forward(tp_ref, groups, share, wgu, wd)
+
+
+def far_kernel(cap, tp_ref, f0, f1, more, pre, bk, wgu, wd, hid, grads, score, b2a, b2b):
+    half, share = b2a.shape
+    relay = f0.shape[1] - share
     rest = jnp.concatenate([wd[:, j + relay : j + share] for j in range(0, wd.shape[1], share)], axis=1)
-    pre[...], back = forward(tp_ref, groups, share, wgu, wd)
-    bk[...] = back + mm(more[...], rest, NT)
-
-
-def far_kernel(cap, tp_ref, f0, f1, pre, bk, wgu, wd, hid, grads, score, b2a, b2b):
-    half, share = b2a.shape
-    start = (pre[...], bk[...])
+    start = (pre[...], bk[...] + mm(more[...], rest, NT))
     hid[...], values, score[...] = units(cap, *forward(tp_ref, ((2, (f0, f1)),), share, wgu, wd, start))
     grads[...] = values
     far = mm(values, wgu[block(tp_ref, 2, share), :], NT).astype(BF16)
@@ -271,49 +281,58 @@
 
     relay = share - 128
     rest = tp * (share - relay)
-    send, more, code, gate, mine = call(
+    send, code, gate, mine = call(
         functools.partial(dispatch_kernel, cap),
-        [shape((rows, share + relay), BF16), shape((rows, rest), BF16), shape((n_tok, experts), F32),
+        [shape((rows, share + relay), BF16), shape((n_tok, experts), F32),
          shape((n_tok, experts), F32), shape((n_tok, share), BF16)],
         unit,
         raw=(0, 1, 2, 3),
     )(me, tokens, out_grad, expert_ids.T, router_t)
+    (more,) = call(
+        functools.partial(direct_kernel, cap, share), [shape((rows, rest), BF16)], unit, scalar=False, raw=(2,)
+    )(code, gate, out_grad)
     own = exchange(send.reshape(peers, cap, share + relay)).reshape(rows, share + relay)
     more = exchange(more.reshape(peers, cap, rest)).reshape(rows, rest)
     pa, nb = hop(own[:half], 1), hop(own[half:], -1)
     pb, na = hop(own[half:], 1), hop(own[:half], -1)
     f0, f1 = hop(pa, 1), hop(nb, -1)
 
-    def load_kernel(wg, wu, wd, wgu_out, wd_out, sems):
-        copies = [
-            pltpu.make_async_copy(wg, wgu_out.at[:, :ff], sems.at[0]),
-            pltpu.make_async_copy(wu, wgu_out.at[:, ff:], sems.at[1]),
-            pltpu.make_async_copy(wd, wd_out, sems.at[2]),
-        ]
-        for copy in copies:
-            copy.start()
-        for copy in copies:
-            copy.wait()
-
-    wgu, wd = pl.pallas_call(
-        load_kernel,
-        out_shape=[pltpu.VMEM((width, 2 * ff), BF16), pltpu.VMEM((ff, width), BF16)],
-        in_specs=[pl.BlockSpec(memory_space=pl.ANY)] * 3,
-        out_specs=[VMEM] * 2,
-        scratch_shapes=[pltpu.SemaphoreType.DMA((3,))],
-        cost_estimate=cost(unit, 4 << 20),
-        compiler_params=pltpu.CompilerParams(vmem_limit_bytes=24 << 20),
-    )(*(pltpu.with_memory_space_constraint(w[0], pltpu.HBM) for w in (w_gate, w_up, w_down)))
-
+    def load(turn):
+        def load_kernel(wg, wu, wd, wgu_out, wd_out, sems):
+            copies = [
+                pltpu.make_async_copy(wg, wgu_out.at[:, :ff], sems.at[0]),
+                pltpu.make_async_copy(wu, wgu_out.at[:, ff:], sems.at[1]),
+                pltpu.make_async_copy(wd, wd_out, sems.at[2]),
+            ]
+            for copy in copies if turn else copies[::-1]:
+                copy.start()
+            for copy in copies:
+                copy.wait()
+
+        return pl.pallas_call(
+            load_kernel,
+            out_shape=[pltpu.VMEM((width, 2 * ff), BF16), pltpu.VMEM((ff, width), BF16)],
+            in_specs=[pl.BlockSpec(memory_space=pl.ANY)] * 3,
+            out_specs=[VMEM] * 2,
+            scratch_shapes=[pltpu.SemaphoreType.DMA((3,))],
+            cost_estimate=cost(unit, 4 << 20),
+            compiler_params=pltpu.CompilerParams(vmem_limit_bytes=24 << 20),
+        )(*(pltpu.with_memory_space_constraint(w[0], pltpu.HBM) for w in (w_gate, w_up, w_down)))
+
+    wgu, wd = load(1)
     near = call(
-        functools.partial(near_kernel, share), [shape((rows, 2 * ff), F32), shape((rows, ff), F32)], 9 * unit, raw=(0,)
-    )(me, own, pa, pb, na, nb, more, wgu, wd)
+        functools.partial(near_kernel, share),
+        [shape((rows, 2 * ff), F32), shape((rows, ff), F32)],
+        9 * unit,
+        raw=(0, 2, 3),
+    )(me, own, pa, pb, na, nb, *load(0))
     hid, grads, score, b2a, b2b = call(
         functools.partial(far_kernel, cap),
         [shape((rows, ff), BF16), shape((rows, 2 * ff), BF16), shape((peers, 128), F32)]
         + [shape((half, share), BF16)] * 2,
         5 * unit,
-    )(me, f0, f1, *near, wgu, wd)
+        raw=(2,),
+    )(me, f0, f1, more, *near, wgu, wd)
     s1, s2 = hop(b2a, 1), hop(b2b, -1)
     b1a, b3b, b0, b1b, b3a = call(
         token_kernel,

time: 167 us -> 170 us (1.018)
  blocking collectives: 38.5 us -> 0 us
  waiting for transfers between devices: 50.3 us -> 71.3 us
  starting transfers between devices: 47.1 us -> 58 us
  Pallas kernels: 25.5 us -> 30.3 us
  local copies, waits for them, and re-layouts: 4.54 us -> 9.12 us
    all_to_all x1 -> x0, blocking collectives: 38.5 us -> none  [exchange(): return lax.all_to_all(value, 'ep', split_axis=0, concat_axis=0, tiled=True)]
    all_to_all x3 -> x4, waiting for transfers between devices: 22.3 us -> 45.6 us  [exchange(): return lax.all_to_all(value, 'ep', split_axis=0, concat_axis=0, tiled=True)]
    all_to_all x3 -> x4, starting transfers between devices: 26 us -> 39.7 us  [exchange(): return lax.all_to_all(value, 'ep', split_axis=0, concat_axis=0, tiled=True)]
    unnamed x16 -> x28, local copies, waits for them, and re-layouts: 3.53 us -> 9.04 us
    ppermute x15, starting transfers between devices: 21.1 us -> 18.3 us  [hop(): return lax.ppermute(value, 'tp', [(i, (i + by) % tp) for i in range(tp)])]
    pallas_call x10 -> x11, Pallas kernels: 23.1 us -> 25.5 us  [run(): pl.pallas_call(body, out_shape=[(pltpu.HBM if i < to_hbm else pltpu.VMEM)...]
    pallas_call x1 -> x2, Pallas kernels: 2.38 us -> 4.77 us  [load(): pl.pallas_call(load_kernel, out_shape=[pltpu.VMEM((width, 2 * ff), BF16),...]
    ppermute x15, waiting for transfers between devices: 28 us -> 25.7 us  [hop(): return lax.ppermute(value, 'tp', [(i, (i + by) % tp) for i in range(tp)])]
  transfers between devices with their start and end apart: 18 -> 19, of which waited for: 9 -> 10; matrix products, arithmetic and copies ran while one was open for 1% -> 0% of each run, Pallas kernels for 10% -> 12%
where the time goes in v3:
time: 170 us
  waiting for transfers between devices  71.3 us (42%)
  starting transfers between devices  58 us (34%)
  Pallas kernels  30.3 us (18%)
  local copies, waits for them, and re-layouts  9.12 us (5%)
    all_to_all x4, waiting for transfers between devices, exchange(): return lax.all_to_all(value, 'ep', split_axis=0, concat_axis=0, tiled=True)  45.6 us
    all_to_all x4, starting transfers between devices, exchange(): return lax.all_to_all(value, 'ep', split_axis=0, concat_axis=0, tiled=True)  39.7 us
    ppermute x15, waiting for transfers between devices, hop(): return lax.ppermute(value, 'tp', [(i, (i + by) % tp) for i in range(tp)])  25.7 us
    pallas_call x11, Pallas kernels, run(): pl.pallas_call(body, out_shape=[(pltpu.HBM if i < to_hbm else pltpu.VMEM)...  25.5 us
    ppermute x15, starting transfers between devices, hop(): return lax.ppermute(value, 'tp', [(i, (i + by) % tp) for i in range(tp)])  18.3 us
    unnamed x28, local copies, waits for them, and re-layouts  9.04 us
    pallas_call x2, Pallas kernels, load(): pl.pallas_call(load_kernel, out_shape=[pltpu.VMEM((width, 2 * ff), BF16),...  4.77 us
  transfers between devices with their start and end apart: 19, of which 10 were waited for; matrix products, arithmetic and copies ran while one was open for 0% of the time, Pallas kernels for 12%

profile of v3, /device:TPU:1, one launch (start us, length us, event | category | flops | bytes accessed | tf_op | source)
XLA Modules:
  0.0 169.5 jit_solution(16737705031741907100)
XLA Ops:
  0.6 3.1 %shard_map.110 = (bf16[512,896]{1,0:T(8,128)(2,1)}, f32[48,64]{1,0:T(8,128)S(1)}, f32[48,64]{1,0:T(8,128)S(1)}, bf16[48,512]{1,0:T(8,128)(2,1)S(1)}) custom-call(s32[1]{0:T(128)} %bitcast.tp_ref, bf16[48,2048]{1,0:T(8,128)(2,1)} %tok_ref.1, bf16[48,2048]{1,0:T(8,128)(2,1)} %og_ref.3, s32[4,48]{1,0:T(4,128)} %bitcast.33, bf16[64,2048]{1,0:T(8,128)(2,1)} %bitcast.31), custom_call_target="tpu_custom_call" | custom-call | flops 201326592 | bytes 4194304 | tf_op jit(solution)/shard_map/pallas_call | solution.py:246
  3.7 13.1 %all-to-all-start = ((bf16[64,8,896]{2,1,0:T(8,128)(2,1)}), bf16[64,8,896]{2,1,0:T(8,128)(2,1)S(1)}, u32[]{:S(2)}, u32[]{:S(2)}) async-start(bf16[64,8,896]{2,1,0:T(8,128)(2,1)} %bitcast.3), calls=%async_computation | async-start | bytes 1835008 | tf_op jit(solution)/shard_map/all_to_all | solution.py:280
  16.8 2.2 %shard_map.111 = bf16[512,512]{1,0:T(8,128)(2,1)} custom-call(f32[48,64]{1,0:T(8,128)S(1)} %get-tuple-element.36.code_ref, f32[48,64]{1,0:T(8,128)S(1)} %get-tuple-element.37.gate_ref.given, bf16[48,2048]{1,0:T(8,128)(2,1)} %og_ref.3), custom_call_target="tpu_custom_call" | custom-call | flops 201326592 | bytes 4194304 | tf_op jit(solution)/shard_map/pallas_call | solution.py:246
  19.1 23.3 %all-to-all-done = bf16[64,8,896]{2,1,0:T(8,128)(2,1)S(1)} async-done(((bf16[64,8,896]{2,1,0:T(8,128)(2,1)}), bf16[64,8,896]{2,1,0:T(8,128)(2,1)S(1)}, u32[]{:S(2)}, u32[]{:S(2)}) %all-to-all-start) | async-done | bytes 917536 | tf_op jit(solution)/shard_map/all_to_all | solution.py:280
  42.4 6.3 %all-to-all-start.1 = ((bf16[64,8,512]{2,1,0:T(8,128)(2,1)}), bf16[64,8,512]{2,1,0:T(8,128)(2,1)}, u32[]{:S(2)}, u32[]{:S(2)}) async-start(bf16[64,8,512]{2,1,0:T(8,128)(2,1)} %bitcast.6), calls=%async_computation.1 | async-start | bytes 1048576 | tf_op jit(solution)/shard_map/all_to_all | solution.py:280
  51.6 2.7 %collective-permute-start.5 = (bf16[256,896]{1,0:T(8,128)(2,1)S(1)}, bf16[256,896]{1,0:T(8,128)(2,1)S(1)}, u32[]{:S(2)}, u32[]{:S(2)}) collective-permute-start(bf16[256,896]{1,0:T(8,128)(2,1)S(1)} %get-tuple-element.66), channel_id=1, source_target_pairs={{0,3},{1,0},{2,1},{3,2},{4,7},{5,4},{6,5},{7,6},{8,11},{9,8},{10,9... | collective-permute-start | bytes 1376264 | tf_op jit(solution)/shard_map/ppermute | solution.py:277
  54.2 7.5 %collective-permute-done.pa = bf16[256,896]{1,0:T(8,128)(2,1)} collective-permute-done((bf16[256,896]{1,0:T(8,128)(2,1)S(1)}, bf16[256,896]{1,0:T(8,128)(2,1)}, u32[]{:S(2)}, u32[]{:S(2)}) %collective-permute-start) | collective-permute-done | bytes 458784 | tf_op jit(solution)/shard_map/ppermute | solution.py:277
  61.7 2.7 %collective-permute-start.3 = (bf16[256,896]{1,0:T(8,128)(2,1)}, bf16[256,896]{1,0:T(8,128)(2,1)}, u32[]{:S(2)}, u32[]{:S(2)}) collective-permute-start(bf16[256,896]{1,0:T(8,128)(2,1)} %collective-permute-done.2.nb), channel_id=1, source_target_pairs={{0,3},{1,0},{2,1},{3,2},{4,7},{5,4},{6,5},{7,6},{8,11},{9,8},{10,9... | collective-permute-start | bytes 1376264 | tf_op jit(solution)/shard_map/ppermute | solution.py:277
  64.4 2.4 %shard_map.112 = (bf16[2048,768]{1,0:T(8,128)(2,1)S(1)}, bf16[384,2048]{1,0:T(8,128)(2,1)S(1)}) custom-call(bf16[2048,384]{1,0:T(8,128)(2,1)} %bitcast.25, bf16[2048,384]{1,0:T(8,128)(2,1)} %bitcast.27, bf16[384,2048]{1,0:T(8,128)(2,1)} %bitcast.29), custom_call_target="tpu_custom_call" | custom-call | flops 201326592 | bytes 4194304 | tf_op jit(solution)/shard_map/pallas_call | solution.py:312
  66.8 2.4 %shard_map.114 = (bf16[2048,768]{1,0:T(8,128)(2,1)S(1)}, bf16[384,2048]{1,0:T(8,128)(2,1)S(1)}) custom-call(bf16[2048,384]{1,0:T(8,128)(2,1)} %bitcast.26, bf16[2048,384]{1,0:T(8,128)(2,1)} %bitcast.28, bf16[384,2048]{1,0:T(8,128)(2,1)} %bitcast.30), custom_call_target="tpu_custom_call" | custom-call | flops 201326592 | bytes 4194304 | tf_op jit(solution)/shard_map/pallas_call | solution.py:312
  72.4 3.8 %shard_map.113 = (f32[512,768]{1,0:T(8,128)S(1)}, f32[512,384]{1,0:T(8,128)S(1)}) custom-call(s32[1]{0:T(128)} %bitcast.tp_ref, bf16[512,896]{1,0:T(8,128)(2,1)} %bitcast.23, bf16[256,896]{1,0:T(8,128)(2,1)} %collective-permute-done.pa, bf16[256,896]{1,0:T(8,128)(2,1)} %copy-done.12, bf16[256,896]{1,0:T(8,128)(2,1)} %copy-done.13, ...), custom_call_target="tpu_custom_call" | custom-call | flops 1811939328 | bytes 4194304 | tf_op jit(solution)/shard_map/pallas_call | solution.py:246
  78.3 3.1 %collective-permute-done.1.f0 = bf16[256,896]{1,0:T(8,128)(2,1)} collective-permute-done((bf16[256,896]{1,0:T(8,128)(2,1)}, bf16[256,896]{1,0:T(8,128)(2,1)}, u32[]{:S(2)}, u32[]{:S(2)}) %collective-permute-start.1) | collective-permute-done | bytes 458784 | tf_op jit(solution)/shard_map/ppermute | solution.py:277
  85.4 3.7 %shard_map.115 = (bf16[512,384]{1,0:T(8,128)(2,1)S(1)}, bf16[512,768]{1,0:T(8,128)(2,1)S(1)}, f32[64,128]{1,0:T(8,128)S(1)}, bf16[256,512]{1,0:T(8,128)(2,1)S(1)}, bf16[256,512]{1,0:T(8,128)(2,1)S(1)}) custom-call(s32[1]{0:T(128)} %bitcast.tp_ref, bf16[256,896]{1,0:T(8,128)(2,1)} %collective-permute-done.1.f0, bf16[256,896]{1,0:T(8,128)(2,1)} %collective-permute-done.3.f1, ...), custom_call_target="tpu_custom_call" | custom-call | flops 1006632960 | bytes 4194304 | tf_op jit(solution)/shard_map/pallas_call | solution.py:246
  90.2 1.7 %collective-permute-start.12 = (bf16[256,512]{1,0:T(8,128)(2,1)S(1)}, bf16[256,512]{1,0:T(8,128)(2,1)S(1)}, u32[]{:S(2)}, u32[]{:S(2)}) collective-permute-start(bf16[256,512]{1,0:T(8,128)(2,1)S(1)} %get-tuple-element.53), channel_id=1, source_target_pairs={{0,3},{1,0},{2,1},{3,2},{4,7},{5,4},{6,5},{7,6},{8,11},{9,8},{10,9... | collective-permute-start | bytes 786440 | tf_op jit(solution)/shard_map/ppermute | solution.py:277
  97.2 2.6 %collective-permute-start.14 = (bf16[256,512]{1,0:T(8,128)(2,1)S(1)}, bf16[256,512]{1,0:T(8,128)(2,1)S(1)}, u32[]{:S(2)}, u32[]{:S(2)}) collective-permute-start(bf16[256,512]{1,0:T(8,128)(2,1)S(1)} %get-tuple-element.55), channel_id=1, source_target_pairs={{0,3},{1,0},{2,1},{3,2},{4,7},{5,4},{6,5},{7,6},{8,11},{9,8},{10,9... | collective-permute-start | bytes 786440 | tf_op jit(solution)/shard_map/ppermute | solution.py:277
  99.8 8.8 %collective-permute-done.6.b = f32[64,128]{1,0:T(8,128)S(1)} collective-permute-done((f32[64,128]{1,0:T(8,128)S(1)}, f32[64,128]{1,0:T(8,128)S(1)}, u32[]{:S(2)}, u32[]{:S(2)}) %collective-permute-start.6) | collective-permute-done | bytes 32800 | tf_op jit(solution)/shard_map/ppermute | solution.py:277
  108.7 1.8 %collective-permute-start.7 = (f32[64,128]{1,0:T(8,128)S(1)}, f32[64,128]{1,0:T(8,128)S(1)}, u32[]{:S(2)}, u32[]{:S(2)}) collective-permute-start(f32[64,128]{1,0:T(8,128)S(1)} %get-tuple-element.44.a), channel_id=1, source_target_pairs={{0,3},{1,0},{2,1},{3,2},{4,7},{5,4},{6,5},{7,6},{8,11},{9,8},{10,9... | collective-permute-start | bytes 98312 | tf_op jit(solution)/shard_map/ppermute | solution.py:277
  112.9 3.0 %collective-permute-done.8.d = f32[64,128]{1,0:T(8,128)S(1)} collective-permute-done((f32[64,128]{1,0:T(8,128)S(1)}, f32[64,128]{1,0:T(8,128)S(1)}, u32[]{:S(2)}, u32[]{:S(2)}) %collective-permute-start.8) | collective-permute-done | bytes 32800 | tf_op jit(solution)/shard_map/ppermute | solution.py:277
  116.5 15.5 %all-to-all-start.2 = ((f32[64,1,128]{2,1,0:T(1,128)}), f32[64,1,128]{2,1,0:T(1,128)S(1)}, u32[]{:S(2)}, u32[]{:S(2)}) async-start(f32[64,1,128]{2,1,0:T(1,128)} %bitcast.13), calls=%async_computation.2 | async-start | bytes 65536 | tf_op jit(solution)/shard_map/all_to_all | solution.py:280
  132.1 9.3 %all-to-all-done.2 = f32[64,1,128]{2,1,0:T(1,128)S(1)} async-done(((f32[64,1,128]{2,1,0:T(1,128)}), f32[64,1,128]{2,1,0:T(1,128)S(1)}, u32[]{:S(2)}, u32[]{:S(2)}) %all-to-all-start.2) | async-done | bytes 32800 | tf_op jit(solution)/shard_map/all_to_all | solution.py:280
  141.4 1.9 %shard_map.120 = (bf16[64,8,640]{2,1,0:T(8,128)(2,1)}, f32[48,64]{1,0:T(8,128)S(1)}) custom-call(f32[64,128]{1,0:T(8,128)S(1)} %bitcast.22, f32[48,64]{1,0:T(8,128)S(1)} %get-tuple-element.36.code_ref, f32[48,64]{1,0:T(8,128)S(1)} %shard_map.117.gate_ref, bf16[48,512]{1,0:T(8,128)(2,1)S(1)} %get-tuple-element.45.tok_ref, f32[512,512]{1,0:T(8,128)S(1)} %copy-done.5, ...), custom_call_target="tpu_custom_call" | custom-call | flops 201326592 | bytes 4194304 | tf_op jit(solution)/shard_map/pallas_call | solution.py:246
  143.3 4.8 %all-to-all-start.3 = ((bf16[64,8,640]{2,1,0:T(8,128)(2,1)}), bf16[64,8,640]{2,1,0:T(8,128)(2,1)S(1)}, u32[]{:S(2)}, u32[]{:S(2)}) async-start(bf16[64,8,640]{2,1,0:T(8,128)(2,1)} %get-tuple-element.56), calls=%async_computation.3 | async-start | bytes 1310720 | tf_op jit(solution)/shard_map/all_to_all | solution.py:280
  148.1 7.5 %shard_map.121 = (bf16[2048,384]{1,0:T(8,128)(2,1)}, bf16[2048,384]{1,0:T(8,128)(2,1)}, bf16[384,2048]{1,0:T(8,128)(2,1)}, f32[48,512]{1,0:T(8,128)S(1)}) custom-call(s32[1]{0:T(128)} %bitcast.tp_ref, bf16[512,896]{1,0:T(8,128)(2,1)} %bitcast.24, bf16[256,896]{1,0:T(8,128)(2,1)} %collective-permute-done.pa, bf16[256,896]{1,0:T(8,128)(2,1)} %copy-done.12, ...), custom_call_target="tpu_custom_call" | custom-call | flops 2415919104 | bytes 4194304 | tf_op jit(solution)/shard_map/pallas_call | solution.py:246
  155.6 13.0 %all-to-all-done.3.home_ref = bf16[64,8,640]{2,1,0:T(8,128)(2,1)S(1)} async-done(((bf16[64,8,640]{2,1,0:T(8,128)(2,1)}), bf16[64,8,640]{2,1,0:T(8,128)(2,1)S(1)}, u32[]{:S(2)}, u32[]{:S(2)}) %all-to-all-start.3) | async-done | bytes 655392 | tf_op jit(solution)/shard_map/all_to_all | solution.py:280
  (56 shorter events, 22.5 us)
Async XLA Ops:
  3.7 38.7 %all-to-all-start = ((bf16[64,8,896]{2,1,0:T(8,128)(2,1)}), bf16[64,8,896]{2,1,0:T(8,128)(2,1)S(1)}, u32[]{:S(2)}, u32[]{:S(2)}) async-start(bf16[64,8,896]{2,1,0:T(8,128)(2,1)} %bitcast.3), calls=%async_computation | async-start | bytes 1835008 | tf_op jit(solution)/shard_map/all_to_all | solution.py:280
  42.4 22.0 %copy-start.11 = (bf16[64,8,896]{2,1,0:T(8,128)(2,1)}, bf16[64,8,896]{2,1,0:T(8,128)(2,1)S(1)}, u32[]{:S(2)}) copy-start(bf16[64,8,896]{2,1,0:T(8,128)(2,1)S(1)} %all-to-all-done) | copy-start | bytes 2752516
  42.4 35.9 %all-to-all-start.1 = ((bf16[64,8,512]{2,1,0:T(8,128)(2,1)}), bf16[64,8,512]{2,1,0:T(8,128)(2,1)}, u32[]{:S(2)}, u32[]{:S(2)}) async-start(bf16[64,8,512]{2,1,0:T(8,128)(2,1)} %bitcast.6), calls=%async_computation.1 | async-start | bytes 1048576 | tf_op jit(solution)/shard_map/all_to_all | solution.py:280
  48.8 12.9 %collective-permute-start = (bf16[256,896]{1,0:T(8,128)(2,1)S(1)}, bf16[256,896]{1,0:T(8,128)(2,1)}, u32[]{:S(2)}, u32[]{:S(2)}) collective-permute-start(bf16[256,896]{1,0:T(8,128)(2,1)S(1)} %get-tuple-element.66), channel_id=1, source_target_pairs={{0,1},{1,2},{2,3},{3,0},{4,5},{5,6},{6,7},{7,4},{8,9},{9,10},{10,1... | collective-permute-start | bytes 1376264 | tf_op jit(solution)/shard_map/ppermute | solution.py:277
  50.1 11.7 %collective-permute-start.2 = (bf16[256,896]{1,0:T(8,128)(2,1)S(1)}, bf16[256,896]{1,0:T(8,128)(2,1)}, u32[]{:S(2)}, u32[]{:S(2)}) collective-permute-start(bf16[256,896]{1,0:T(8,128)(2,1)S(1)} %get-tuple-element.65), channel_id=1, source_target_pairs={{0,3},{1,0},{2,1},{3,2},{4,7},{5,4},{6,5},{7,6},{8,11},{9,8},{10,9... | collective-permute-start | bytes 1376264 | tf_op jit(solution)/shard_map/ppermute | solution.py:277
  51.6 19.9 %collective-permute-start.4 = (bf16[256,896]{1,0:T(8,128)(2,1)S(1)}, bf16[256,896]{1,0:T(8,128)(2,1)S(1)}, u32[]{:S(2)}, u32[]{:S(2)}) collective-permute-start(bf16[256,896]{1,0:T(8,128)(2,1)S(1)} %get-tuple-element.65), channel_id=1, source_target_pairs={{0,1},{1,2},{2,3},{3,0},{4,5},{5,6},{6,7},{7,4},{8,9},{9,10},{10,1... | collective-permute-start | bytes 1376264 | tf_op jit(solution)/shard_map/ppermute | solution.py:277
  51.6 19.9 %collective-permute-start.5 = (bf16[256,896]{1,0:T(8,128)(2,1)S(1)}, bf16[256,896]{1,0:T(8,128)(2,1)S(1)}, u32[]{:S(2)}, u32[]{:S(2)}) collective-permute-start(bf16[256,896]{1,0:T(8,128)(2,1)S(1)} %get-tuple-element.66), channel_id=1, source_target_pairs={{0,3},{1,0},{2,1},{3,2},{4,7},{5,4},{6,5},{7,6},{8,11},{9,8},{10,9... | collective-permute-start | bytes 1376264 | tf_op jit(solution)/shard_map/ppermute | solution.py:277
  61.7 19.7 %collective-permute-start.1 = (bf16[256,896]{1,0:T(8,128)(2,1)}, bf16[256,896]{1,0:T(8,128)(2,1)}, u32[]{:S(2)}, u32[]{:S(2)}) collective-permute-start(bf16[256,896]{1,0:T(8,128)(2,1)} %collective-permute-done.pa), channel_id=1, source_target_pairs={{0,1},{1,2},{2,3},{3,0},{4,5},{5,6},{6,7},{7,4},{8,9},{9,10},{10,1... | collective-permute-start | bytes 1376264 | tf_op jit(solution)/shard_map/ppermute | solution.py:277
  61.7 19.7 %collective-permute-start.3 = (bf16[256,896]{1,0:T(8,128)(2,1)}, bf16[256,896]{1,0:T(8,128)(2,1)}, u32[]{:S(2)}, u32[]{:S(2)}) collective-permute-start(bf16[256,896]{1,0:T(8,128)(2,1)} %collective-permute-done.2.nb), channel_id=1, source_target_pairs={{0,3},{1,0},{2,1},{3,2},{4,7},{5,4},{6,5},{7,6},{8,11},{9,8},{10,9... | collective-permute-start | bytes 1376264 | tf_op jit(solution)/shard_map/ppermute | solution.py:277
  89.0 4.6 %copy-start.8 = (bf16[512,768]{1,0:T(8,128)(2,1)}, bf16[512,768]{1,0:T(8,128)(2,1)S(1)}, u32[]{:S(2)}) copy-start(bf16[512,768]{1,0:T(8,128)(2,1)S(1)} %get-tuple-element.46.grads_ref.grads) | copy-start | bytes 2359300
  89.0 4.6 %copy-start.9 = (bf16[512,384]{1,0:T(8,128)(2,1)}, bf16[512,384]{1,0:T(8,128)(2,1)S(1)}, u32[]{:S(2)}) copy-start(bf16[512,384]{1,0:T(8,128)(2,1)S(1)} %get-tuple-element.57.hid) | copy-start | bytes 1179652
  89.0 7.9 %collective-permute-start.11 = (bf16[256,512]{1,0:T(8,128)(2,1)S(1)}, bf16[256,512]{1,0:T(8,128)(2,1)S(1)}, u32[]{:S(2)}, u32[]{:S(2)}) collective-permute-start(bf16[256,512]{1,0:T(8,128)(2,1)S(1)} %get-tuple-element.51), channel_id=1, source_target_pairs={{0,1},{1,2},{2,3},{3,0},{4,5},{5,6},{6,7},{7,4},{8,9},{9,10},{10,1... | collective-permute-start | bytes 786440 | tf_op jit(solution)/shard_map/ppermute | solution.py:277
  90.2 6.8 %collective-permute-start.12 = (bf16[256,512]{1,0:T(8,128)(2,1)S(1)}, bf16[256,512]{1,0:T(8,128)(2,1)S(1)}, u32[]{:S(2)}, u32[]{:S(2)}) collective-permute-start(bf16[256,512]{1,0:T(8,128)(2,1)S(1)} %get-tuple-element.53), channel_id=1, source_target_pairs={{0,3},{1,0},{2,1},{3,2},{4,7},{5,4},{6,5},{7,6},{8,11},{9,8},{10,9... | collective-permute-start | bytes 786440 | tf_op jit(solution)/shard_map/ppermute | solution.py:277
  94.6 46.8 %copy-start.5 = (f32[512,512]{1,0:T(8,128)S(1)}, f32[512,512]{1,0:T(8,128)}, u32[]{:S(2)}) copy-start(f32[512,512]{1,0:T(8,128)} %copy-done.4) | copy-start | bytes 3145732
  94.6 46.8 %collective-permute-start.10 = (bf16[256,512]{1,0:T(8,128)(2,1)}, bf16[256,512]{1,0:T(8,128)(2,1)S(1)}, u32[]{:S(2)}, u32[]{:S(2)}) collective-permute-start(bf16[256,512]{1,0:T(8,128)(2,1)} %get-tuple-element.49), channel_id=1, source_target_pairs={{0,3},{1,0},{2,1},{3,2},{4,7},{5,4},{6,5},{7,6},{8,11},{9,8},{10,9... | collective-permute-start | bytes 786440 | tf_op jit(solution)/shard_map/ppermute | solution.py:277
  95.8 45.6 %collective-permute-start.9 = (bf16[256,512]{1,0:T(8,128)(2,1)S(1)}, bf16[256,512]{1,0:T(8,128)(2,1)S(1)}, u32[]{:S(2)}, u32[]{:S(2)}) collective-permute-start(bf16[256,512]{1,0:T(8,128)(2,1)S(1)} %get-tuple-element.48), channel_id=1, source_target_pairs={{0,1},{1,2},{2,3},{3,0},{4,5},{5,6},{6,7},{7,4},{8,9},{9,10},{10,1... | collective-permute-start | bytes 786440 | tf_op jit(solution)/shard_map/ppermute | solution.py:277
  97.1 44.3 %collective-permute-start.13 = (bf16[256,512]{1,0:T(8,128)(2,1)S(1)}, bf16[256,512]{1,0:T(8,128)(2,1)S(1)}, u32[]{:S(2)}, u32[]{:S(2)}) collective-permute-start(bf16[256,512]{1,0:T(8,128)(2,1)S(1)} %get-tuple-element.54), channel_id=1, source_target_pairs={{0,1},{1,2},{2,3},{3,0},{4,5},{5,6},{6,7},{7,4},{8,9},{9,10},{10,1... | collective-permute-start | bytes 786440 | tf_op jit(solution)/shard_map/ppermute | solution.py:277
  97.2 44.2 %collective-permute-start.14 = (bf16[256,512]{1,0:T(8,128)(2,1)S(1)}, bf16[256,512]{1,0:T(8,128)(2,1)S(1)}, u32[]{:S(2)}, u32[]{:S(2)}) collective-permute-start(bf16[256,512]{1,0:T(8,128)(2,1)S(1)} %get-tuple-element.55), channel_id=1, source_target_pairs={{0,3},{1,0},{2,1},{3,2},{4,7},{5,4},{6,5},{7,6},{8,11},{9,8},{10,9... | collective-permute-start | bytes 786440 | tf_op jit(solution)/shard_map/ppermute | solution.py:277
  99.8 8.8 %collective-permute-start.6 = (f32[64,128]{1,0:T(8,128)S(1)}, f32[64,128]{1,0:T(8,128)S(1)}, u32[]{:S(2)}, u32[]{:S(2)}) collective-permute-start(f32[64,128]{1,0:T(8,128)S(1)} %get-tuple-element.44.a), channel_id=1, source_target_pairs={{0,1},{1,2},{2,3},{3,0},{4,5},{5,6},{6,7},{7,4},{8,9},{9,10},{10,1... | collective-permute-start | bytes 98312 | tf_op jit(solution)/shard_map/ppermute | solution.py:277
  108.7 3.0 %collective-permute-start.7 = (f32[64,128]{1,0:T(8,128)S(1)}, f32[64,128]{1,0:T(8,128)S(1)}, u32[]{:S(2)}, u32[]{:S(2)}) collective-permute-start(f32[64,128]{1,0:T(8,128)S(1)} %get-tuple-element.44.a), channel_id=1, source_target_pairs={{0,3},{1,0},{2,1},{3,2},{4,7},{5,4},{6,5},{7,6},{8,11},{9,8},{10,9... | collective-permute-start | bytes 98312 | tf_op jit(solution)/shard_map/ppermute | solution.py:277
  111.6 4.3 %collective-permute-start.8 = (f32[64,128]{1,0:T(8,128)S(1)}, f32[64,128]{1,0:T(8,128)S(1)}, u32[]{:S(2)}, u32[]{:S(2)}) collective-permute-start(f32[64,128]{1,0:T(8,128)S(1)} %get-tuple-element.44.a), channel_id=1, source_target_pairs={{0,2},{1,3},{2,0},{3,1},{4,6},{5,7},{6,4},{7,5},{8,10},{9,11},{10,... | collective-permute-start | bytes 98312 | tf_op jit(solution)/shard_map/ppermute | solution.py:277
  116.5 24.8 %all-to-all-start.2 = ((f32[64,1,128]{2,1,0:T(1,128)}), f32[64,1,128]{2,1,0:T(1,128)S(1)}, u32[]{:S(2)}, u32[]{:S(2)}) async-start(f32[64,1,128]{2,1,0:T(1,128)} %bitcast.13), calls=%async_computation.2 | async-start | bytes 65536 | tf_op jit(solution)/shard_map/all_to_all | solution.py:280
  143.3 4.8 %copy-start.10 = (f32[48,64]{1,0:T(8,128)}, f32[48,64]{1,0:T(8,128)S(1)}, u32[]{:S(2)}) copy-start(f32[48,64]{1,0:T(8,128)S(1)} %get-tuple-element.58.d_logits_ref) | copy-start | bytes 36868
  143.3 25.2 %all-to-all-start.3 = ((bf16[64,8,640]{2,1,0:T(8,128)(2,1)}), bf16[64,8,640]{2,1,0:T(8,128)(2,1)S(1)}, u32[]{:S(2)}, u32[]{:S(2)}) async-start(bf16[64,8,640]{2,1,0:T(8,128)(2,1)} %get-tuple-element.56), calls=%async_computation.3 | async-start | bytes 1310720 | tf_op jit(solution)/shard_map/all_to_all | solution.py:280
  (9 other events, 9.9 us)

commit v4 on v3

--- a/solution.py
+++ b/solution.py
@@ -189,14 +189,7 @@
         gwd_ref[:, pl.ds(at.start, relay)] = mm(hid[...], joined(refs, slice(share, None)), TN).astype(BF16)
 
 
-def router_kernel(cap, q_ref, code_ref, gate_ref, tok_ref, *refs):
-    (b0, d1, d2, e1, e2), (payload_ref, d_logits_ref) = refs[:5], refs[5:]
-    rows, share = b0.shape
-    half = rows // 2
-    for i, (near, far) in enumerate(((d2, e1), (d1, e2))):
-        n = half // cap
-        value = b0[i * half : (i + 1) * half] + near[...].astype(F32) + far[...].astype(F32)
-        payload_ref[pl.ds(i * n, n), :, :share] = value.astype(BF16).reshape(n, cap, share)
+def router_kernel(cap, q_ref, code_ref, gate_ref, tok_ref, term_ref, d_logits_ref):
     code, gate = code_ref[...], gate_ref[...]
     q = q_ref[...].T
     score = jnp.zeros_like(code)
@@ -207,10 +200,20 @@
     term = mm(d_logits, tok_ref[...].astype(F32), TN, HI)
     high = term.astype(BF16)
     low = (term - high.astype(F32)).astype(BF16)
-    pieces = share // 128
+    pieces = term.shape[1] // 128
     for j in range(pieces):
-        payload_ref[:, j, share:] = high[:, j * 128 : (j + 1) * 128]
-        payload_ref[:, pieces + j, share:] = low[:, j * 128 : (j + 1) * 128]
+        term_ref[:, j, :] = high[:, j * 128 : (j + 1) * 128]
+        term_ref[:, pieces + j, :] = low[:, j * 128 : (j + 1) * 128]
+
+
+def pack_kernel(cap, b0, d1, d2, e1, e2, term_ref, payload_ref):
+    rows, share = b0.shape
+    half = rows // 2
+    for i, (near, far) in enumerate(((d2, e1), (d1, e2))):
+        n = half // cap
+        value = b0[i * half : (i + 1) * half] + near[...].astype(F32) + far[...].astype(F32)
+        payload_ref[pl.ds(i * n, n), :, :share] = value.astype(BF16).reshape(n, cap, share)
+    payload_ref[:, :, share:] = term_ref[...]
 
 
 def mark_kernel(given, out):
@@ -297,42 +300,45 @@
     pb, na = hop(own[half:], 1), hop(own[:half], -1)
     f0, f1 = hop(pa, 1), hop(nb, -1)
 
-    def load(turn):
-        def load_kernel(wg, wu, wd, wgu_out, wd_out, sems):
+    def load(*others):
+        arrays = [w_gate[0], w_up[0], w_down[0], *others]
+
+        def load_kernel(*refs):
+            (wg, wu, *sources), (wgu_out, *targets), sems = refs[: len(arrays)], refs[len(arrays) : -1], refs[-1]
             copies = [
                 pltpu.make_async_copy(wg, wgu_out.at[:, :ff], sems.at[0]),
                 pltpu.make_async_copy(wu, wgu_out.at[:, ff:], sems.at[1]),
-                pltpu.make_async_copy(wd, wd_out, sems.at[2]),
             ]
-            for copy in copies if turn else copies[::-1]:
+            for i, (source, target) in enumerate(zip(sources, targets)):
+                copies.append(pltpu.make_async_copy(source, target, sems.at[2 + i]))
+            for copy in copies:
                 copy.start()
             for copy in copies:
                 copy.wait()
 
         return pl.pallas_call(
             load_kernel,
-            out_shape=[pltpu.VMEM((width, 2 * ff), BF16), pltpu.VMEM((ff, width), BF16)],
-            in_specs=[pl.BlockSpec(memory_space=pl.ANY)] * 3,
-            out_specs=[VMEM] * 2,
-            scratch_shapes=[pltpu.SemaphoreType.DMA((3,))],
+            out_shape=[pltpu.VMEM((width, 2 * ff), BF16)] + [pltpu.VMEM(a.shape, a.dtype) for a in arrays[2:]],
+            in_specs=[pl.BlockSpec(memory_space=pl.ANY)] * len(arrays),
+            out_specs=[VMEM] * (len(arrays) - 1),
+            scratch_shapes=[pltpu.SemaphoreType.DMA((len(arrays),))],
             cost_estimate=cost(unit, 4 << 20),
             compiler_params=pltpu.CompilerParams(vmem_limit_bytes=24 << 20),
-        )(*(pltpu.with_memory_space_constraint(w[0], pltpu.HBM) for w in (w_gate, w_up, w_down)))
-
-    wgu, wd = load(1)
+        )(*(pltpu.with_memory_space_constraint(a, pltpu.HBM) for a in arrays))
+
+    wgu, wd, more_near = load(more)
     near = call(
         functools.partial(near_kernel, share),
         [shape((rows, 2 * ff), F32), shape((rows, ff), F32)],
         9 * unit,
         raw=(0, 2, 3),
-    )(me, own, pa, pb, na, nb, *load(0))
+    )(me, own, pa, pb, na, nb, *load())
     hid, grads, score, b2a, b2b = call(
         functools.partial(far_kernel, cap),
         [shape((rows, ff), BF16), shape((rows, 2 * ff), BF16), shape((peers, 128), F32)]
         + [shape((half, share), BF16)] * 2,
         5 * unit,
-        raw=(2,),
-    )(me, f0, f1, more, *near, wgu, wd)
+    )(me, f0, f1, more_near, *near, wgu, wd)
     s1, s2 = hop(b2a, 1), hop(b2b, -1)
     b1a, b3b, b0, b1b, b3a = call(
         token_kernel,
@@ -347,12 +353,15 @@
         score, hop(score, 1), hop(score, -1), hop(score, 2)
     )
     q = exchange(score.reshape(peers, 1, 128)).reshape(peers, 128)
-    payload, d_logits = call(
+    term, d_logits = call(
         functools.partial(router_kernel, cap),
-        [shape((peers, cap, share + 128), BF16), shape((n_tok, experts), F32)],
+        [shape((peers, cap, 128), BF16), shape((n_tok, experts), F32)],
         unit,
         scalar=False,
-    )(q, code, gate, mine, b0, d1, d2, e1, e2)
+    )(q, code, gate, mine)
+    (payload,) = call(
+        functools.partial(pack_kernel, cap), [shape((peers, cap, share + 128), BF16)], unit, scalar=False
+    )(b0, d1, d2, e1, e2, term)
     home = exchange(payload)
     gwg, gwu, gwd, part = call(
         functools.partial(weight_kernel, share),

time: 170 us -> 168 us (0.988)
  local copies, waits for them, and re-layouts: 9.12 us -> 2.16 us
  starting transfers between devices: 58 us -> 60.5 us
  waiting for transfers between devices: 71.3 us -> 73.5 us
    unnamed x28 -> x12, local copies, waits for them, and re-layouts: 9.04 us -> 1.16 us
    ppermute x15, starting transfers between devices: 18.3 us -> 22.1 us  [hop(): return lax.ppermute(value, 'tp', [(i, (i + by) % tp) for i in range(tp)])]
    ppermute x15, waiting for transfers between devices: 25.7 us -> 27.9 us  [hop(): return lax.ppermute(value, 'tp', [(i, (i + by) % tp) for i in range(tp)])]
    pallas_call x11 -> x12, Pallas kernels: 25.5 us -> 25 us  [run(): pl.pallas_call(body, out_shape=[(pltpu.HBM if i < to_hbm else pltpu.VMEM)...]
  transfers between devices with their start and end apart: 19 -> 19, of which waited for: 10 -> 11; matrix products, arithmetic and copies ran while one was open for 0% -> 1% of each run, Pallas kernels for 12% -> 13%
where the time goes in v4:
time: 168 us; the launch traced here: 167 us
  waiting for transfers between devices  73.5 us (44%)
  starting transfers between devices  60.5 us (36%)
  Pallas kernels  30 us (18%)
  local copies, waits for them, and re-layouts  2.16 us (1%)
    all_to_all x4, waiting for transfers between devices, exchange(): return lax.all_to_all(value, 'ep', split_axis=0, concat_axis=0, tiled=True)  45.6 us
    all_to_all x4, starting transfers between devices, exchange(): return lax.all_to_all(value, 'ep', split_axis=0, concat_axis=0, tiled=True)  38.5 us
    ppermute x15, waiting for transfers between devices, hop(): return lax.ppermute(value, 'tp', [(i, (i + by) % tp) for i in range(tp)])  27.9 us
    pallas_call x12, Pallas kernels, run(): pl.pallas_call(body, out_shape=[(pltpu.HBM if i < to_hbm else pltpu.VMEM)...  25 us
    ppermute x15, starting transfers between devices, hop(): return lax.ppermute(value, 'tp', [(i, (i + by) % tp) for i in range(tp)])  22.1 us
    pallas_call x2, Pallas kernels, load(): pl.pallas_call(load_kernel, out_shape=[pltpu.VMEM((width, 2 * ff), BF16)]...  5 us
  transfers between devices with their start and end apart: 19, of which 11 were waited for; matrix products, arithmetic and copies ran while one was open for 1% of the time, Pallas kernels for 13%

profile of v4, /device:TPU:1, one launch (start us, length us, event | category | flops | bytes accessed | tf_op | source)
XLA Modules:
  0.0 167.0 jit_solution(13415223256000467860)
XLA Ops:
  0.6 3.1 %shard_map.110 = (bf16[512,896]{1,0:T(8,128)(2,1)}, f32[48,64]{1,0:T(8,128)S(1)}, f32[48,64]{1,0:T(8,128)S(1)}, bf16[48,512]{1,0:T(8,128)(2,1)S(1)}) custom-call(s32[1]{0:T(128)} %bitcast.tp_ref, bf16[48,2048]{1,0:T(8,128)(2,1)} %tok_ref.1, bf16[48,2048]{1,0:T(8,128)(2,1)} %og_ref.3, s32[4,48]{1,0:T(4,128)} %bitcast.33, bf16[64,2048]{1,0:T(8,128)(2,1)} %bitcast.31), custom_call_target="tpu_custom_call" | custom-call | flops 201326592 | bytes 4194304 | tf_op jit(solution)/shard_map/pallas_call | solution.py:249
  3.7 13.1 %all-to-all-start = ((bf16[64,8,896]{2,1,0:T(8,128)(2,1)}), bf16[64,8,896]{2,1,0:T(8,128)(2,1)S(1)}, u32[]{:S(2)}, u32[]{:S(2)}) async-start(bf16[64,8,896]{2,1,0:T(8,128)(2,1)} %bitcast.3), calls=%async_computation | async-start | bytes 1835008 | tf_op jit(solution)/shard_map/all_to_all | solution.py:283
  19.1 23.3 %all-to-all-done = bf16[64,8,896]{2,1,0:T(8,128)(2,1)S(1)} async-done(((bf16[64,8,896]{2,1,0:T(8,128)(2,1)}), bf16[64,8,896]{2,1,0:T(8,128)(2,1)S(1)}, u32[]{:S(2)}, u32[]{:S(2)}) %all-to-all-start) | async-done | bytes 917536 | tf_op jit(solution)/shard_map/all_to_all | solution.py:283
  42.4 6.3 %all-to-all-start.1 = ((bf16[64,8,512]{2,1,0:T(8,128)(2,1)}), bf16[64,8,512]{2,1,0:T(8,128)(2,1)}, u32[]{:S(2)}, u32[]{:S(2)}) async-start(bf16[64,8,512]{2,1,0:T(8,128)(2,1)} %bitcast.9), calls=%async_computation.1 | async-start | bytes 1048576 | tf_op jit(solution)/shard_map/all_to_all | solution.py:283
  52.4 2.5 %collective-permute-start.5 = (bf16[256,896]{1,0:T(8,128)(2,1)}, bf16[256,896]{1,0:T(8,128)(2,1)}, u32[]{:S(2)}, u32[]{:S(2)}) collective-permute-start(bf16[256,896]{1,0:T(8,128)(2,1)} %get-tuple-element.68), channel_id=1, source_target_pairs={{0,3},{1,0},{2,1},{3,2},{4,7},{5,4},{6,5},{7,6},{8,11},{9,8},{10,9... | collective-permute-start | bytes 1376264 | tf_op jit(solution)/shard_map/ppermute | solution.py:280
  54.9 7.0 %collective-permute-done.2.nb = bf16[256,896]{1,0:T(8,128)(2,1)} collective-permute-done((bf16[256,896]{1,0:T(8,128)(2,1)}, bf16[256,896]{1,0:T(8,128)(2,1)}, u32[]{:S(2)}, u32[]{:S(2)}) %collective-permute-start.2) | collective-permute-done | bytes 458784 | tf_op jit(solution)/shard_map/ppermute | solution.py:280
  61.9 3.4 %collective-permute-start.3 = (bf16[256,896]{1,0:T(8,128)(2,1)}, bf16[256,896]{1,0:T(8,128)(2,1)}, u32[]{:S(2)}, u32[]{:S(2)}) collective-permute-start(bf16[256,896]{1,0:T(8,128)(2,1)} %collective-permute-done.2.nb), channel_id=1, source_target_pairs={{0,3},{1,0},{2,1},{3,2},{4,7},{5,4},{6,5},{7,6},{8,11},{9,8},{10,9... | collective-permute-start | bytes 1376264 | tf_op jit(solution)/shard_map/ppermute | solution.py:280
  68.8 2.6 %shard_map.112 = (bf16[2048,768]{1,0:T(8,128)(2,1)S(1)}, bf16[384,2048]{1,0:T(8,128)(2,1)S(1)}, bf16[512,512]{1,0:T(8,128)(2,1)S(1)}) custom-call(bf16[2048,384]{1,0:T(8,128)(2,1)} %bitcast.26, bf16[2048,384]{1,0:T(8,128)(2,1)} %bitcast.28, bf16[384,2048]{1,0:T(8,128)(2,1)} %bitcast.30, bf16[512,512]{1,0:T(8,128)(2,1)} %bitcast.10.refs_3_.more), custom_call_target="tpu_custom_call" | custom-call | flops 201326592 | bytes 4194304 | tf_op jit(solution)/shard_map/pallas_call | solution.py:319
  71.4 3.4 %collective-permute-done.4.pb = bf16[256,896]{1,0:T(8,128)(2,1)} collective-permute-done((bf16[256,896]{1,0:T(8,128)(2,1)}, bf16[256,896]{1,0:T(8,128)(2,1)}, u32[]{:S(2)}, u32[]{:S(2)}) %collective-permute-start.4) | collective-permute-done | bytes 458784 | tf_op jit(solution)/shard_map/ppermute | solution.py:280
  74.8 3.8 %shard_map.114 = (f32[512,768]{1,0:T(8,128)S(1)}, f32[512,384]{1,0:T(8,128)S(1)}) custom-call(s32[1]{0:T(128)} %bitcast.tp_ref, bf16[512,896]{1,0:T(8,128)(2,1)} %bitcast.23, bf16[256,896]{1,0:T(8,128)(2,1)} %collective-permute-done.pa, bf16[256,896]{1,0:T(8,128)(2,1)} %collective-permute-done.4.pb, bf16[256,896]{1,0:T(8,128)(2,1)} %collective-permute-done.5.na, ...), custom_call_target="tpu_custom_call" | custom-call | flops 1811939328 | bytes 4194304 | tf_op jit(solution)/shard_map/pallas_call | solution.py:249
  78.7 2.9 %collective-permute-done.3.f1 = bf16[256,896]{1,0:T(8,128)(2,1)} collective-permute-done((bf16[256,896]{1,0:T(8,128)(2,1)}, bf16[256,896]{1,0:T(8,128)(2,1)}, u32[]{:S(2)}, u32[]{:S(2)}) %collective-permute-start.3) | collective-permute-done | bytes 458784 | tf_op jit(solution)/shard_map/ppermute | solution.py:280
  81.5 3.1 %collective-permute-done.1.f0 = bf16[256,896]{1,0:T(8,128)(2,1)} collective-permute-done((bf16[256,896]{1,0:T(8,128)(2,1)}, bf16[256,896]{1,0:T(8,128)(2,1)}, u32[]{:S(2)}, u32[]{:S(2)}) %collective-permute-start.1) | collective-permute-done | bytes 458784 | tf_op jit(solution)/shard_map/ppermute | solution.py:280
  84.7 3.5 %shard_map.115 = (bf16[512,384]{1,0:T(8,128)(2,1)S(1)}, bf16[512,768]{1,0:T(8,128)(2,1)S(1)}, f32[64,128]{1,0:T(8,128)S(1)}, bf16[256,512]{1,0:T(8,128)(2,1)S(1)}, bf16[256,512]{1,0:T(8,128)(2,1)S(1)}) custom-call(s32[1]{0:T(128)} %bitcast.tp_ref, bf16[256,896]{1,0:T(8,128)(2,1)} %collective-permute-done.1.f0, bf16[256,896]{1,0:T(8,128)(2,1)} %collective-permute-done.3.f1, ...), custom_call_target="tpu_custom_call" | custom-call | flops 1006632960 | bytes 4194304 | tf_op jit(solution)/shard_map/pallas_call | solution.py:249
  88.5 2.7 %collective-permute-start.9 = (bf16[256,512]{1,0:T(8,128)(2,1)S(1)}, bf16[256,512]{1,0:T(8,128)(2,1)S(1)}, u32[]{:S(2)}, u32[]{:S(2)}) collective-permute-start(bf16[256,512]{1,0:T(8,128)(2,1)S(1)} %get-tuple-element.53), channel_id=1, source_target_pairs={{0,3},{1,0},{2,1},{3,2},{4,7},{5,4},{6,5},{7,6},{8,11},{9,8},{10,9... | collective-permute-start | bytes 786440 | tf_op jit(solution)/shard_map/ppermute | solution.py:280
  92.7 2.7 %collective-permute-start.7 = (bf16[256,512]{1,0:T(8,128)(2,1)S(1)}, bf16[256,512]{1,0:T(8,128)(2,1)S(1)}, u32[]{:S(2)}, u32[]{:S(2)}) collective-permute-start(bf16[256,512]{1,0:T(8,128)(2,1)S(1)} %get-tuple-element.49), channel_id=1, source_target_pairs={{0,3},{1,0},{2,1},{3,2},{4,7},{5,4},{6,5},{7,6},{8,11},{9,8},{10,9... | collective-permute-start | bytes 786440 | tf_op jit(solution)/shard_map/ppermute | solution.py:280
  96.1 2.7 %collective-permute-start.11 = (bf16[256,512]{1,0:T(8,128)(2,1)S(1)}, bf16[256,512]{1,0:T(8,128)(2,1)S(1)}, u32[]{:S(2)}, u32[]{:S(2)}) collective-permute-start(bf16[256,512]{1,0:T(8,128)(2,1)S(1)} %get-tuple-element.55), channel_id=1, source_target_pairs={{0,3},{1,0},{2,1},{3,2},{4,7},{5,4},{6,5},{7,6},{8,11},{9,8},{10,9... | collective-permute-start | bytes 786440 | tf_op jit(solution)/shard_map/ppermute | solution.py:280
  99.6 5.8 %collective-permute-done.14.d = f32[64,128]{1,0:T(8,128)S(1)} collective-permute-done((f32[64,128]{1,0:T(8,128)S(1)}, f32[64,128]{1,0:T(8,128)S(1)}, u32[]{:S(2)}, u32[]{:S(2)}) %collective-permute-start.14) | collective-permute-done | bytes 32800 | tf_op jit(solution)/shard_map/ppermute | solution.py:280
  105.4 4.1 %collective-permute-start.13 = (f32[64,128]{1,0:T(8,128)S(1)}, f32[64,128]{1,0:T(8,128)S(1)}, u32[]{:S(2)}, u32[]{:S(2)}) collective-permute-start(f32[64,128]{1,0:T(8,128)S(1)} %get-tuple-element.56.a), channel_id=1, source_target_pairs={{0,3},{1,0},{2,1},{3,2},{4,7},{5,4},{6,5},{7,6},{8,11},{9,8},{10,9... | collective-permute-start | bytes 98312 | tf_op jit(solution)/shard_map/ppermute | solution.py:280
  110.6 4.2 %collective-permute-done.12.b = f32[64,128]{1,0:T(8,128)S(1)} collective-permute-done((f32[64,128]{1,0:T(8,128)S(1)}, f32[64,128]{1,0:T(8,128)S(1)}, u32[]{:S(2)}, u32[]{:S(2)}) %collective-permute-start.12) | collective-permute-done | bytes 32800 | tf_op jit(solution)/shard_map/ppermute | solution.py:280
  115.4 14.3 %all-to-all-start.2 = ((f32[64,1,128]{2,1,0:T(1,128)}), f32[64,1,128]{2,1,0:T(1,128)S(1)}, u32[]{:S(2)}, u32[]{:S(2)}) async-start(f32[64,1,128]{2,1,0:T(1,128)} %bitcast.13), calls=%async_computation.2 | async-start | bytes 65536 | tf_op jit(solution)/shard_map/all_to_all | solution.py:283
  129.7 9.3 %all-to-all-done.2 = f32[64,1,128]{2,1,0:T(1,128)S(1)} async-done(((f32[64,1,128]{2,1,0:T(1,128)}), f32[64,1,128]{2,1,0:T(1,128)S(1)}, u32[]{:S(2)}, u32[]{:S(2)}) %all-to-all-start.2) | async-done | bytes 32800 | tf_op jit(solution)/shard_map/all_to_all | solution.py:283
  140.9 4.8 %all-to-all-start.3 = ((bf16[64,8,640]{2,1,0:T(8,128)(2,1)}), bf16[64,8,640]{2,1,0:T(8,128)(2,1)S(1)}, u32[]{:S(2)}, u32[]{:S(2)}) async-start(bf16[64,8,640]{2,1,0:T(8,128)(2,1)} %shard_map.121), calls=%async_computation.3 | async-start | bytes 1310720 | tf_op jit(solution)/shard_map/all_to_all | solution.py:283
  145.6 7.5 %shard_map.122 = (bf16[2048,384]{1,0:T(8,128)(2,1)}, bf16[2048,384]{1,0:T(8,128)(2,1)}, bf16[384,2048]{1,0:T(8,128)(2,1)}, f32[48,512]{1,0:T(8,128)S(1)}) custom-call(s32[1]{0:T(128)} %bitcast.tp_ref, bf16[512,896]{1,0:T(8,128)(2,1)} %bitcast.24, bf16[256,896]{1,0:T(8,128)(2,1)} %collective-permute-done.pa, bf16[256,896]{1,0:T(8,128)(2,1)} %collective-permute-done.4.pb, ...), custom_call_target="tpu_custom_call" | custom-call | flops 2415919104 | bytes 4194304 | tf_op jit(solution)/shard_map/pallas_call | solution.py:249
  153.1 13.0 %all-to-all-done.3.home_ref = bf16[64,8,640]{2,1,0:T(8,128)(2,1)S(1)} async-done(((bf16[64,8,640]{2,1,0:T(8,128)(2,1)}), bf16[64,8,640]{2,1,0:T(8,128)(2,1)S(1)}, u32[]{:S(2)}, u32[]{:S(2)}) %all-to-all-start.3) | async-done | bytes 655392 | tf_op jit(solution)/shard_map/all_to_all | solution.py:283
  (41 shorter events, 17.3 us)
Async XLA Ops:
  3.7 38.7 %all-to-all-start = ((bf16[64,8,896]{2,1,0:T(8,128)(2,1)}), bf16[64,8,896]{2,1,0:T(8,128)(2,1)S(1)}, u32[]{:S(2)}, u32[]{:S(2)}) async-start(bf16[64,8,896]{2,1,0:T(8,128)(2,1)} %bitcast.3), calls=%async_computation | async-start | bytes 1835008 | tf_op jit(solution)/shard_map/all_to_all | solution.py:283
  42.4 22.9 %copy-start.5 = (bf16[64,8,896]{2,1,0:T(8,128)(2,1)}, bf16[64,8,896]{2,1,0:T(8,128)(2,1)S(1)}, u32[]{:S(2)}) copy-start(bf16[64,8,896]{2,1,0:T(8,128)(2,1)S(1)} %all-to-all-done) | copy-start | bytes 2752516
  42.4 26.4 %all-to-all-start.1 = ((bf16[64,8,512]{2,1,0:T(8,128)(2,1)}), bf16[64,8,512]{2,1,0:T(8,128)(2,1)}, u32[]{:S(2)}, u32[]{:S(2)}) async-start(bf16[64,8,512]{2,1,0:T(8,128)(2,1)} %bitcast.9), calls=%async_computation.1 | async-start | bytes 1048576 | tf_op jit(solution)/shard_map/all_to_all | solution.py:283
  49.7 12.1 %collective-permute-start.2 = (bf16[256,896]{1,0:T(8,128)(2,1)}, bf16[256,896]{1,0:T(8,128)(2,1)}, u32[]{:S(2)}, u32[]{:S(2)}) collective-permute-start(bf16[256,896]{1,0:T(8,128)(2,1)} %get-tuple-element.67), channel_id=1, source_target_pairs={{0,3},{1,0},{2,1},{3,2},{4,7},{5,4},{6,5},{7,6},{8,11},{9,8},{10,9... | collective-permute-start | bytes 1376264 | tf_op jit(solution)/shard_map/ppermute | solution.py:280
  52.2 13.1 %collective-permute-start = (bf16[256,896]{1,0:T(8,128)(2,1)}, bf16[256,896]{1,0:T(8,128)(2,1)}, u32[]{:S(2)}, u32[]{:S(2)}) collective-permute-start(bf16[256,896]{1,0:T(8,128)(2,1)} %get-tuple-element.68), channel_id=1, source_target_pairs={{0,1},{1,2},{2,3},{3,0},{4,5},{5,6},{6,7},{7,4},{8,9},{9,10},{10,1... | collective-permute-start | bytes 1376264 | tf_op jit(solution)/shard_map/ppermute | solution.py:280
  52.2 22.6 %collective-permute-start.4 = (bf16[256,896]{1,0:T(8,128)(2,1)}, bf16[256,896]{1,0:T(8,128)(2,1)}, u32[]{:S(2)}, u32[]{:S(2)}) collective-permute-start(bf16[256,896]{1,0:T(8,128)(2,1)} %get-tuple-element.67), channel_id=1, source_target_pairs={{0,1},{1,2},{2,3},{3,0},{4,5},{5,6},{6,7},{7,4},{8,9},{9,10},{10,1... | collective-permute-start | bytes 1376264 | tf_op jit(solution)/shard_map/ppermute | solution.py:280
  52.4 22.4 %collective-permute-start.5 = (bf16[256,896]{1,0:T(8,128)(2,1)}, bf16[256,896]{1,0:T(8,128)(2,1)}, u32[]{:S(2)}, u32[]{:S(2)}) collective-permute-start(bf16[256,896]{1,0:T(8,128)(2,1)} %get-tuple-element.68), channel_id=1, source_target_pairs={{0,3},{1,0},{2,1},{3,2},{4,7},{5,4},{6,5},{7,6},{8,11},{9,8},{10,9... | collective-permute-start | bytes 1376264 | tf_op jit(solution)/shard_map/ppermute | solution.py:280
  61.9 19.7 %collective-permute-start.3 = (bf16[256,896]{1,0:T(8,128)(2,1)}, bf16[256,896]{1,0:T(8,128)(2,1)}, u32[]{:S(2)}, u32[]{:S(2)}) collective-permute-start(bf16[256,896]{1,0:T(8,128)(2,1)} %collective-permute-done.2.nb), channel_id=1, source_target_pairs={{0,3},{1,0},{2,1},{3,2},{4,7},{5,4},{6,5},{7,6},{8,11},{9,8},{10,9... | collective-permute-start | bytes 1376264 | tf_op jit(solution)/shard_map/ppermute | solution.py:280
  65.3 19.4 %collective-permute-start.1 = (bf16[256,896]{1,0:T(8,128)(2,1)}, bf16[256,896]{1,0:T(8,128)(2,1)}, u32[]{:S(2)}, u32[]{:S(2)}) collective-permute-start(bf16[256,896]{1,0:T(8,128)(2,1)} %collective-permute-done.pa), channel_id=1, source_target_pairs={{0,1},{1,2},{2,3},{3,0},{4,5},{5,6},{6,7},{7,4},{8,9},{9,10},{10,1... | collective-permute-start | bytes 1376264 | tf_op jit(solution)/shard_map/ppermute | solution.py:280
  67.7 1.1 copy-start
  68.8 6.0 %copy-start.1 = (bf16[384,2048]{1,0:T(8,128)(2,1)S(1)}, bf16[384,2048]{1,0:T(8,128)(2,1)}, u32[]{:S(2)}) copy-start(bf16[384,2048]{1,0:T(8,128)(2,1)} %copy-done) | copy-start | bytes 4718596
  88.2 4.4 %copy-start.2 = (bf16[512,768]{1,0:T(8,128)(2,1)}, bf16[512,768]{1,0:T(8,128)(2,1)S(1)}, u32[]{:S(2)}) copy-start(bf16[512,768]{1,0:T(8,128)(2,1)S(1)} %get-tuple-element.46.grads_ref.grads) | copy-start | bytes 2359300
  88.2 4.4 %copy-start.3 = (bf16[512,384]{1,0:T(8,128)(2,1)}, bf16[512,384]{1,0:T(8,128)(2,1)S(1)}, u32[]{:S(2)}) copy-start(bf16[512,384]{1,0:T(8,128)(2,1)S(1)} %get-tuple-element.59.hid) | copy-start | bytes 1179652
  88.2 7.7 %collective-permute-start.8 = (bf16[256,512]{1,0:T(8,128)(2,1)S(1)}, bf16[256,512]{1,0:T(8,128)(2,1)S(1)}, u32[]{:S(2)}, u32[]{:S(2)}) collective-permute-start(bf16[256,512]{1,0:T(8,128)(2,1)S(1)} %get-tuple-element.51), channel_id=1, source_target_pairs={{0,1},{1,2},{2,3},{3,0},{4,5},{5,6},{6,7},{7,4},{8,9},{9,10},{10,1... | collective-permute-start | bytes 786440 | tf_op jit(solution)/shard_map/ppermute | solution.py:280
  88.5 7.4 %collective-permute-start.9 = (bf16[256,512]{1,0:T(8,128)(2,1)S(1)}, bf16[256,512]{1,0:T(8,128)(2,1)S(1)}, u32[]{:S(2)}, u32[]{:S(2)}) collective-permute-start(bf16[256,512]{1,0:T(8,128)(2,1)S(1)} %get-tuple-element.53), channel_id=1, source_target_pairs={{0,3},{1,0},{2,1},{3,2},{4,7},{5,4},{6,5},{7,6},{8,11},{9,8},{10,9... | collective-permute-start | bytes 786440 | tf_op jit(solution)/shard_map/ppermute | solution.py:280
  92.6 47.2 %collective-permute-start.6 = (bf16[256,512]{1,0:T(8,128)(2,1)}, bf16[256,512]{1,0:T(8,128)(2,1)S(1)}, u32[]{:S(2)}, u32[]{:S(2)}) collective-permute-start(bf16[256,512]{1,0:T(8,128)(2,1)} %get-tuple-element.48), channel_id=1, source_target_pairs={{0,1},{1,2},{2,3},{3,0},{4,5},{5,6},{6,7},{7,4},{8,9},{9,10},{10,1... | collective-permute-start | bytes 786440 | tf_op jit(solution)/shard_map/ppermute | solution.py:280
  92.7 47.2 %collective-permute-start.7 = (bf16[256,512]{1,0:T(8,128)(2,1)S(1)}, bf16[256,512]{1,0:T(8,128)(2,1)S(1)}, u32[]{:S(2)}, u32[]{:S(2)}) collective-permute-start(bf16[256,512]{1,0:T(8,128)(2,1)S(1)} %get-tuple-element.49), channel_id=1, source_target_pairs={{0,3},{1,0},{2,1},{3,2},{4,7},{5,4},{6,5},{7,6},{8,11},{9,8},{10,9... | collective-permute-start | bytes 786440 | tf_op jit(solution)/shard_map/ppermute | solution.py:280
  96.0 43.9 %collective-permute-start.10 = (bf16[256,512]{1,0:T(8,128)(2,1)S(1)}, bf16[256,512]{1,0:T(8,128)(2,1)S(1)}, u32[]{:S(2)}, u32[]{:S(2)}) collective-permute-start(bf16[256,512]{1,0:T(8,128)(2,1)S(1)} %get-tuple-element.54), channel_id=1, source_target_pairs={{0,1},{1,2},{2,3},{3,0},{4,5},{5,6},{6,7},{7,4},{8,9},{9,10},{10,1... | collective-permute-start | bytes 786440 | tf_op jit(solution)/shard_map/ppermute | solution.py:280
  96.1 43.8 %collective-permute-start.11 = (bf16[256,512]{1,0:T(8,128)(2,1)S(1)}, bf16[256,512]{1,0:T(8,128)(2,1)S(1)}, u32[]{:S(2)}, u32[]{:S(2)}) collective-permute-start(bf16[256,512]{1,0:T(8,128)(2,1)S(1)} %get-tuple-element.55), channel_id=1, source_target_pairs={{0,3},{1,0},{2,1},{3,2},{4,7},{5,4},{6,5},{7,6},{8,11},{9,8},{10,9... | collective-permute-start | bytes 786440 | tf_op jit(solution)/shard_map/ppermute | solution.py:280
  98.7 6.7 %collective-permute-start.14 = (f32[64,128]{1,0:T(8,128)S(1)}, f32[64,128]{1,0:T(8,128)S(1)}, u32[]{:S(2)}, u32[]{:S(2)}) collective-permute-start(f32[64,128]{1,0:T(8,128)S(1)} %get-tuple-element.56.a), channel_id=1, source_target_pairs={{0,2},{1,3},{2,0},{3,1},{4,6},{5,7},{6,4},{7,5},{8,10},{9,11},{10,... | collective-permute-start | bytes 98312 | tf_op jit(solution)/shard_map/ppermute | solution.py:280
  105.4 5.1 %collective-permute-start.13 = (f32[64,128]{1,0:T(8,128)S(1)}, f32[64,128]{1,0:T(8,128)S(1)}, u32[]{:S(2)}, u32[]{:S(2)}) collective-permute-start(f32[64,128]{1,0:T(8,128)S(1)} %get-tuple-element.56.a), channel_id=1, source_target_pairs={{0,3},{1,0},{2,1},{3,2},{4,7},{5,4},{6,5},{7,6},{8,11},{9,8},{10,9... | collective-permute-start | bytes 98312 | tf_op jit(solution)/shard_map/ppermute | solution.py:280
  110.5 4.3 %collective-permute-start.12 = (f32[64,128]{1,0:T(8,128)S(1)}, f32[64,128]{1,0:T(8,128)S(1)}, u32[]{:S(2)}, u32[]{:S(2)}) collective-permute-start(f32[64,128]{1,0:T(8,128)S(1)} %get-tuple-element.56.a), channel_id=1, source_target_pairs={{0,1},{1,2},{2,3},{3,0},{4,5},{5,6},{6,7},{7,4},{8,9},{9,10},{10,1... | collective-permute-start | bytes 98312 | tf_op jit(solution)/shard_map/ppermute | solution.py:280
  115.4 23.6 %all-to-all-start.2 = ((f32[64,1,128]{2,1,0:T(1,128)}), f32[64,1,128]{2,1,0:T(1,128)S(1)}, u32[]{:S(2)}, u32[]{:S(2)}) async-start(f32[64,1,128]{2,1,0:T(1,128)} %bitcast.13), calls=%async_computation.2 | async-start | bytes 65536 | tf_op jit(solution)/shard_map/all_to_all | solution.py:283
  140.9 25.2 %all-to-all-start.3 = ((bf16[64,8,640]{2,1,0:T(8,128)(2,1)}), bf16[64,8,640]{2,1,0:T(8,128)(2,1)S(1)}, u32[]{:S(2)}, u32[]{:S(2)}) async-start(bf16[64,8,640]{2,1,0:T(8,128)(2,1)} %shard_map.121), calls=%async_computation.3 | async-start | bytes 1310720 | tf_op jit(solution)/shard_map/all_to_all | solution.py:283
  (1 other events, 1.1 us)
